TPU v7x, 256 devices: a whole 4x4x8 slice. The times are simulated.
256 devices in a mesh: sp: 128 (over z, y, x), tp: 2 (over core).
Axes of the slice: x: 4, y: 4, z: 8, core: 2. Of those that a mesh axis runs over, the one named last changes fastest.
Arguments:
- conv_value: bfloat16 [65536, 1536], P('sp', 'tp'), may hold values from -6 to 6
- conv_gate: bfloat16 [65536, 1536], P('sp', 'tp'), may hold values from -8 to 8
- conv_out: bfloat16 [65536, 1536], P('sp', 'tp'), may hold values from -40 to 40
- conv_taps: bfloat16 [31, 1536], P(None, 'tp'), may hold values from -1 to 1
- norm_gain: float32 [1536], P('tp'), may hold values from 0.1 to 1.9
- norm_shift: float32 [1536], P('tp'), may hold values from -3 to 3
- proj_weight: bfloat16 [2048, 1536], P(None, 'tp'), may hold values from -0.15625 to 0.15625
- out_grad: bfloat16 [65536, 2048], P('sp'), may hold values from -24 to 24
Outputs:
- grad_value: bfloat16 [65536, 1536], P('sp', 'tp')
- grad_gate: bfloat16 [65536, 1536], P('sp', 'tp')
- grad_taps: float32 [31, 1536], P(None, 'tp')
- grad_gain: float32 [1536], P('tp')
- grad_shift: float32 [1536], P('tp')
- grad_proj: float32 [2048, 1536], P('sp', 'tp')
All inputs are finite; a program needn't handle non-finite values.
Results may differ from a plain program's by a relative error of at most 0.005.
Values may be sent and summed in bfloat16 or wider, within the bound.
A program may use at most 64 MiB of HBM per device.

v0:
```python
import functools

import jax
import jax.numpy as jnp
from jax import lax
from jax.experimental import pallas as pl
from jax.experimental.pallas import tpu as pltpu
from jax.sharding import PartitionSpec as P

norm_eps = 1e-05
MESH = pl.DeviceIdType.MESH
F32 = jnp.float32
BF16 = jnp.bfloat16
LANES = 128


def repeat(start, stop, body, unroll):
    assert (stop - start) % unroll == 0

    def step(i, carry):
        for u in range(unroll):
            body(start + i * unroll + u, carry)
        return carry

    lax.fori_loop(0, (stop - start) // unroll, step, 0)


def bit(x, b):
    return lax.rem(x // (1 << b), 2)


def coordinate_bits(index, nbits):
    bits = [bit(index, b) for b in range(nbits)]
    if nbits >= 2:
        bits[nbits - 2] = lax.rem(bits[nbits - 2] + bits[nbits - 1], 2)
    return bits


def partner_of(me, b, nbits):
    def flip(x, c):
        return x + (1 << c) * (1 - 2 * bit(me, c))

    other = flip(me, b)
    if nbits >= 2 and b == nbits - 1:
        other = flip(other, b - 1)
    return other


def stage_orders(nbits, groups):
    body = list(range(max(nbits - 1, 1)))
    tail = list(range(len(body), nbits))
    return [body[g % len(body):] + body[: g % len(body)] + tail for g in range(groups)]


def kernel(
    dims,
    cv_hbm, cg_hbm, co_hbm, taps_ref, gain_ref, shift_ref, w_hbm, og_hbm,
    gv_hbm, gg_hbm, small_out, proj_out,
    cv, cg, co, w, og, ogt, active, normed, dsilu, scaled, hgx, gv, gg,
    st_a, st_b, st_d, pk_a, pk_b, pk_c, pk_d, tapf, acc, sendbuf, recvbuf, tapacc, rowacc, flat, parts, mine, whole,
    in_sem, out_sem, tp_send, tp_recv, halo_send, halo_recv,
    rs_send, rs_recv, a_send, a_recv, b_send, b_recv,
):
    n, nbits, groups, chan_total = dims
    rows, chan = co.shape
    width = og.shape[1]
    block = width // n
    gcols = chan // groups
    cblocks = chan // LANES
    ntaps = taps_ref.shape[0]
    reach = ntaps - 1
    halo = hgx.shape[1] - rows
    chunk = mine.shape[0]
    per = small_out.shape[0]
    me = lax.axis_index("sp")
    core = lax.axis_index("tp")
    other_core = 1 - core
    orders = stage_orders(nbits, groups)

    loads = [
        pltpu.make_async_copy(src, dst, in_sem.at[i])
        for i, (src, dst) in enumerate(
            ((co_hbm, co), (og_hbm, og), (w_hbm, w), (cg_hbm, cg), (cv_hbm, cv))
        )
    ]
    loads[0].start()

    barrier = pltpu.get_barrier_semaphore()

    def greet(i, carry):
        pl.semaphore_signal(
            barrier, inc=1, device_id=(lax.rem(me + i, n), core), device_id_type=MESH
        )
        return carry

    lax.fori_loop(1, n, greet, 0)
    pl.semaphore_signal(barrier, inc=1, device_id=(me, other_core), device_id_type=MESH)

    lane_low = lax.broadcasted_iota(jnp.int32, (1, LANES), 1) < LANES // 2

    gain = gain_ref[...].reshape(1, chan)
    shift = shift_ref[...].reshape(1, chan)
    nt = rows // LANES
    mid = LANES // 2

    def pack(dst):
        for t in range(nt):
            turned = st_a[t * LANES:(t + 1) * LANES, :].T
            dst[0, t:t + 1, :] = turned[:1, :]
            dst[1, t:t + 1, :] = turned[mid:mid + 1, :]

    def unpack(packed, dst):
        for t in range(nt):
            dst[t * LANES:(t + 1) * LANES, :] = jnp.broadcast_to(packed[t:t + 1, :], (LANES, LANES)).T

    def wide(x):
        return jnp.concatenate([x] * cblocks, axis=1)

    loads[0].wait()
    for copy in loads[1:]:
        copy.start()

    def stats(i, carry):
        at = pl.ds(pl.multiple_of(i * 64, 64), 64)
        h = co[at, :].astype(F32)
        mean = jnp.sum(h, axis=1, keepdims=True) / chan
        d = h - mean
        m2 = jnp.sum(d * d, axis=1, keepdims=True)
        st_a[at, :] = jnp.where(lane_low, mean, m2)
        return carry

    repeat(0, rows // 64, stats, 2)
    pack(pk_a)
    pl.semaphore_wait(barrier, n)
    swap_a = pltpu.make_async_remote_copy(
        src_ref=pk_a, dst_ref=pk_b, send_sem=tp_send.at[0], recv_sem=tp_recv.at[0],
        device_id=(me, other_core), device_id_type=MESH,
    )
    swap_a.start()

    loads[1].wait()
    mybits = coordinate_bits(me, nbits)
    sub = LANES // block

    def transpose(c, carry):
        t = og[:, pl.ds(pl.multiple_of(c * LANES, LANES), LANES)].T
        for s in range(sub):
            rbits = coordinate_bits(c * sub + s, nbits)
            piece = t[s * block:(s + 1) * block, :]
            for g in range(groups):
                place = 0
                for k, b in enumerate(orders[g]):
                    place = place + lax.rem(rbits[b] + mybits[b], 2) * (1 << (nbits - 1 - k))
                ogt[g, place] = piece
        return carry

    lax.fori_loop(0, width // LANES, transpose, 0)

    swap_a.wait()
    gap = pk_a[0] - pk_b[0]
    variance = (pk_a[1] + pk_b[1] + gap * gap * (0.5 * chan)) / chan_total
    unpack(0.5 * (pk_a[0] + pk_b[0]), st_b)
    unpack(lax.rsqrt(variance + norm_eps), st_d)

    def norm(i, carry):
        at = pl.ds(pl.multiple_of(i * 32, 32), 32)
        z = (co[at, :].astype(F32) - wide(st_b[at, :])) * wide(st_d[at, :])
        normed[at, :] = z
        x = z * gain + shift
        sig = jax.nn.sigmoid(x)
        active[at, :] = (x * sig).astype(BF16)
        dsilu[at, :] = sig * (1.0 + x * (1.0 - sig))
        return carry

    repeat(0, rows // 32, norm, 2)

    def stage_copy(g, k):
        count = n >> (k + 1)
        off = n - (n >> k)
        return pltpu.make_async_remote_copy(
            src_ref=sendbuf.at[g, pl.ds(off, count)],
            dst_ref=recvbuf.at[g, pl.ds(off, count)],
            send_sem=rs_send.at[g, k],
            recv_sem=rs_recv.at[g, k],
            device_id=(partner_of(me, orders[g][k], nbits), core),
            device_id_type=MESH,
        )

    unit = max(1, n // 4)

    def product(g, start):
        lhs = ogt[g, pl.ds(start, unit)].reshape(unit * block, rows)
        out = jnp.dot(lhs, active[:, g * gcols:(g + 1) * gcols], preferred_element_type=F32)
        return out.reshape(unit, block, gcols)

    for g in range(groups):

        def far(i, carry, g=g):
            sendbuf[g, pl.ds(i * unit, unit)] = product(g, n // 2 + i * unit).astype(BF16)
            return carry

        lax.fori_loop(0, n // 2 // unit, far, 0)
        stage_copy(g, 0).start()
    def stage(k):
        count = n >> (k + 1)
        off = n - (n >> k)
        for g in range(groups):
            stage_copy(g, k).wait_recv()
            if k + 1 < nbits:
                keep = count // 2

                def pass_on(i, carry, g=g):
                    sendbuf[g, off + count + i] = (
                        acc[g, keep + i] + recvbuf[g, off + keep + i].astype(F32)
                    ).astype(BF16)
                    return carry

                lax.fori_loop(0, count - keep, pass_on, 0)
                stage_copy(g, k + 1).start()
            else:
                keep = count

            def take(i, carry, g=g):
                acc[g, i] = acc[g, i] + recvbuf[g, off + i].astype(F32)
                return carry

            lax.fori_loop(0, keep, take, 0)

    loads[2].wait()
    rowacc[...] = jnp.zeros_like(rowacc)

    def act(i, carry):
        at = pl.ds(pl.multiple_of(i * 128, 128), 128)
        scaled[at, :] = jnp.dot(og[at, :], w[...], preferred_element_type=F32)
        return carry

    lax.fori_loop(0, rows // 128, act, 0)

    def grads(i, carry):
        at = pl.ds(pl.multiple_of(i * 32, 32), 32)
        z = normed[at, :]
        ng = scaled[at, :] * dsilu[at, :]
        ngz = ng * z
        rowacc[0] = rowacc[0] + jnp.sum(ngz.reshape(4, 8, chan), axis=0)
        rowacc[1] = rowacc[1] + jnp.sum(ng.reshape(4, 8, chan), axis=0)
        s = ng * gain
        scaled[at, :] = s
        total = jnp.sum(s, axis=1, keepdims=True)
        dot = jnp.sum(s * z, axis=1, keepdims=True)
        st_a[at, :] = jnp.where(lane_low, total, dot)
        return carry

    repeat(0, rows // 32, grads, 2)
    pack(pk_c)
    swap_b = pltpu.make_async_remote_copy(
        src_ref=pk_c, dst_ref=pk_d, send_sem=tp_send.at[1], recv_sem=tp_recv.at[1],
        device_id=(me, other_core), device_id_type=MESH,
    )
    swap_b.start()
    tapacc[...] = jnp.zeros_like(tapacc)
    for c in range(cblocks):
        tapf[c] = taps_ref[:, c * LANES:(c + 1) * LANES].astype(F32)
    flat[...] = jnp.zeros_like(flat)
    for g in range(groups):

        def near(i, carry, g=g):
            acc[g, pl.ds(i * unit, unit)] = product(g, i * unit)
            return carry

        lax.fori_loop(0, n // 2 // unit, near, 0)

    swap_b.wait()
    unpack((pk_c[0] + pk_d[0]) / chan_total, st_a)
    unpack((pk_c[1] + pk_d[1]) / chan_total, st_b)

    def height(i, carry):
        at = pl.ds(pl.multiple_of(i * 32, 32), 32)
        hg = wide(st_d[at, :]) * (
            scaled[at, :] - wide(st_a[at, :]) - normed[at, :] * wide(st_b[at, :])
        )
        for c in range(cblocks):
            hgx[c, at, :] = hg[:, c * LANES:(c + 1) * LANES]
        return carry

    height(0, 0)
    halo_copy = pltpu.make_async_remote_copy(
        src_ref=hgx.at[:, pl.ds(0, halo)],
        dst_ref=hgx.at[:, pl.ds(rows, halo)],
        send_sem=halo_send, recv_sem=halo_recv,
        device_id=(lax.rem(me + n - 1, n), core), device_id_type=MESH,
    )

    @pl.when(me > 0)
    def _():
        halo_copy.start()

    repeat(1, rows // 32, height, 3)

    @pl.when(me == n - 1)
    def _():
        hgx[:, rows:, :] = jnp.zeros((cblocks, halo, LANES), F32)

    loads[3].wait()
    loads[4].wait()
    stage(0)

    @pl.when(me < n - 1)
    def _():
        halo_copy.wait_recv()

    step = 64
    steps = rows // step

    def conv(i, carry):
        c = i // steps
        r = pl.multiple_of(lax.rem(i, steps) * step, step)
        at = pl.ds(r, step)
        cols = pl.ds(pl.multiple_of(c * LANES, LANES), LANES)
        sig = jax.nn.sigmoid(cg[at, cols].astype(F32))
        value = cv[at, cols].astype(F32)
        gated = (value * sig).astype(BF16).astype(F32)
        total = jnp.zeros((step, LANES), F32)
        for j in range(ntaps):
            h = hgx[c, pl.ds(r + reach - j, step), :]
            total = total + tapf[c, pl.ds(j, 1), :] * h
            tapacc[c, j] = tapacc[c, j] + jnp.sum((gated * h).reshape(step // 8, 8, LANES), axis=0)
        gv[at, cols] = (total * sig).astype(BF16)
        gg[at, cols] = (total * value * sig * (1.0 - sig)).astype(BF16)
        return carry

    cut = cblocks * steps * 3 // 4
    lax.fori_loop(0, cut, conv, 0)
    stage(1)
    lax.fori_loop(cut, cblocks * steps, conv, 0)

    stores = [
        pltpu.make_async_copy(src, dst, out_sem.at[i])
        for i, (src, dst) in enumerate(((gv, gv_hbm), (gg, gg_hbm)))
    ]
    for copy in stores:
        copy.start()

    for c in range(cblocks):
        rowsum = jnp.sum(tapacc[c], axis=1)
        flat[c * per:c * per + ntaps, :] = rowsum
        for j in range(2):
            flat[c * per + ntaps + j:c * per + ntaps + j + 1, :] = jnp.sum(
                rowacc[j, :, c * LANES:(c + 1) * LANES], axis=0, keepdims=True
            )

    def spread(i):
        peer = lax.rem(me + i, n)
        return pltpu.make_async_remote_copy(
            src_ref=flat.at[pl.ds(pl.multiple_of(peer * chunk, chunk), chunk)],
            dst_ref=parts.at[me],
            send_sem=a_send.at[peer], recv_sem=a_recv.at[me],
            device_id=(peer, core), device_id_type=MESH,
        )

    def collect(i):
        peer = lax.rem(me + i, n)
        return pltpu.make_async_remote_copy(
            src_ref=mine,
            dst_ref=whole.at[pl.ds(pl.multiple_of(me * chunk, chunk), chunk)],
            send_sem=b_send.at[peer], recv_sem=b_recv.at[me],
            device_id=(peer, core), device_id_type=MESH,
        )

    def arrived_part(peer):
        return pltpu.make_async_remote_copy(
            src_ref=flat.at[pl.ds(pl.multiple_of(peer * chunk, chunk), chunk)],
            dst_ref=parts.at[peer],
            send_sem=a_send.at[peer], recv_sem=a_recv.at[peer],
            device_id=(peer, core), device_id_type=MESH,
        )

    def arrived_whole(peer):
        return pltpu.make_async_remote_copy(
            src_ref=mine,
            dst_ref=whole.at[pl.ds(pl.multiple_of(peer * chunk, chunk), chunk)],
            send_sem=b_send.at[peer], recv_sem=b_recv.at[peer],
            device_id=(peer, core), device_id_type=MESH,
        )

    def loop(body):
        def run(i, carry):
            body(i)
            return carry

        lax.fori_loop(1, n, run, 0)

    loop(lambda i: spread(i).start())
    mine[...] = flat[pl.ds(pl.multiple_of(me * chunk, chunk), chunk), :]

    for k in range(2, nbits - 1):
        stage(k)

    def add_part(i):
        peer = lax.rem(me + i, n)
        arrived_part(peer).wait_recv()
        mine[...] = mine[...] + parts[peer]

    loop(add_part)
    loop(lambda i: collect(i).start())
    whole[pl.ds(pl.multiple_of(me * chunk, chunk), chunk), :] = mine[...]

    stage(nbits - 1)
    for g in range(groups):
        proj_out[:, g * gcols:(g + 1) * gcols] = acc[g, 0]
    loop(lambda i: arrived_whole(lax.rem(me + i, n)).wait_recv())
    for c in range(cblocks):
        small_out[:, c * LANES:(c + 1) * LANES] = whole[c * per:(c + 1) * per, :]

    loop(lambda i: arrived_part(lax.rem(me + i, n)).wait_send())
    loop(lambda i: arrived_whole(lax.rem(me + i, n)).wait_send())
    for g in range(groups):
        for k in range(nbits):
            stage_copy(g, k).wait_send()

    @pl.when(me > 0)
    def _():
        halo_copy.wait_send()

    for copy in stores:
        copy.wait()


def place(gv_in, gg_in, small, proj_in, gv_out, gg_out, taps, gain, shift, proj_out, gv, gg, proj, in_sem, out_sem):
    ins = [
        pltpu.make_async_copy(src, dst, in_sem.at[i])
        for i, (src, dst) in enumerate(((gv_in, gv), (gg_in, gg), (proj_in, proj)))
    ]
    outs = [
        pltpu.make_async_copy(src, dst, out_sem.at[i])
        for i, (src, dst) in enumerate(((gv, gv_out), (gg, gg_out), (proj, proj_out)))
    ]
    for copy in ins:
        copy.start()
    ntaps = taps.shape[0]
    taps[...] = small[:ntaps, :]
    gain[...] = small[ntaps, :]
    shift[...] = small[ntaps + 1, :]
    for came, goes in zip(ins, outs):
        came.wait()
        goes.start()
    for copy in outs:
        copy.wait()


def local(conv_value, conv_gate, conv_out, conv_taps, norm_gain, norm_shift, proj_weight, out_grad):
    rows, chan = conv_value.shape
    ntaps = conv_taps.shape[0]
    width = out_grad.shape[1]
    n = lax.axis_size("sp")
    nbits = n.bit_length() - 1
    assert 1 << nbits == n and lax.axis_size("tp") == 2
    groups = 3
    gcols = chan // groups
    block = width // n
    cblocks = chan // LANES
    halo = 32
    per = -(-(ntaps + 2) // 8) * 8
    chunk = -(-(-(-per * cblocks // n)) // 8) * 8
    dims = (n, nbits, groups, chan * 2)
    hbm = pl.BlockSpec(memory_space=pl.ANY)
    vmem = pl.BlockSpec(memory_space=pltpu.VMEM)
    dma = pltpu.SemaphoreType.DMA
    grad_value, grad_gate, small, grad_proj = pl.pallas_call(
        functools.partial(kernel, dims),
        out_shape=(
            jax.ShapeDtypeStruct((rows, chan), BF16),
            jax.ShapeDtypeStruct((rows, chan), BF16),
            jax.ShapeDtypeStruct((per, chan), F32),
            jax.ShapeDtypeStruct((block, chan), F32),
        ),
        in_specs=[hbm, hbm, hbm, vmem, vmem, vmem, hbm, hbm],
        out_specs=(hbm, hbm, vmem, vmem),
        scratch_shapes=[
            pltpu.VMEM((rows, chan), BF16),
            pltpu.VMEM((rows, chan), BF16),
            pltpu.VMEM((rows, chan), BF16),
            pltpu.VMEM((width, chan), BF16),
            pltpu.VMEM((rows, width), BF16),
            pltpu.VMEM((groups, n, block, rows), BF16),
            pltpu.VMEM((rows, chan), BF16),
            pltpu.VMEM((rows, chan), F32),
            pltpu.VMEM((rows, chan), F32),
            pltpu.VMEM((rows, chan), F32),
            pltpu.VMEM((cblocks, rows + halo, LANES), F32),
            pltpu.VMEM((rows, chan), BF16),
            pltpu.VMEM((rows, chan), BF16),
            pltpu.VMEM((rows, LANES), F32),
            pltpu.VMEM((rows, LANES), F32),
            pltpu.VMEM((rows, LANES), F32),
            *[pltpu.VMEM((2, rows // LANES, LANES), F32)] * 4,
            pltpu.VMEM((cblocks, ntaps, LANES), F32),
            pltpu.VMEM((groups, n // 2, block, gcols), F32),
            pltpu.VMEM((groups, n, block, gcols), BF16),
            pltpu.VMEM((groups, n, block, gcols), BF16),
            pltpu.VMEM((cblocks, ntaps, 8, LANES), F32),
            pltpu.VMEM((2, 8, chan), F32),
            pltpu.VMEM((n * chunk, LANES), F32),
            pltpu.VMEM((n, chunk, LANES), F32),
            pltpu.VMEM((chunk, LANES), F32),
            pltpu.VMEM((n * chunk, LANES), F32),
            dma((5,)), dma((2,)),
            dma((2,)), dma((2,)),
            dma, dma,
            dma((groups, nbits)), dma((groups, nbits)),
            dma((n,)), dma((n,)),
            dma((n,)), dma((n,)),
        ],
        compiler_params=pltpu.CompilerParams(
            collective_id=0, has_side_effects=True, vmem_limit_bytes=60 * 1024 * 1024
        ),
    )(
        conv_value, conv_gate, conv_out, conv_taps, norm_gain, norm_shift, proj_weight, out_grad,
    )
    return pl.pallas_call(
        place,
        out_shape=(
            jax.ShapeDtypeStruct((rows, chan), BF16),
            jax.ShapeDtypeStruct((rows, chan), BF16),
            jax.ShapeDtypeStruct((ntaps, chan), F32),
            jax.ShapeDtypeStruct((chan,), F32),
            jax.ShapeDtypeStruct((chan,), F32),
            jax.ShapeDtypeStruct((block, chan), F32),
        ),
        in_specs=[hbm, hbm, vmem, hbm],
        out_specs=(hbm, hbm, vmem, vmem, vmem, hbm),
        scratch_shapes=[
            pltpu.VMEM((rows, chan), BF16),
            pltpu.VMEM((rows, chan), BF16),
            pltpu.VMEM((block, chan), F32),
            dma((3,)), dma((3,)),
        ],
    )(grad_value, grad_gate, small, grad_proj)


def solution(mesh):
    in_specs = (
        P("sp", "tp"),
        P("sp", "tp"),
        P("sp", "tp"),
        P(None, "tp"),
        P("tp"),
        P("tp"),
        P(None, "tp"),
        P("sp", None),
    )
    out_specs = (P("sp", "tp"), P("sp", "tp"), P(None, "tp"), P("tp"), P("tp"), P("sp", "tp"))
    return jax.shard_map(local, mesh=mesh, in_specs=in_specs, out_specs=out_specs, check_vma=False)
```

profile of v0, /device:TPU:8, one launch (start us, length us, event | category | flops | bytes accessed | tf_op | source)
XLA Modules:
  0.0 111.7 jit_solution(10549398447779514613)
XLA Ops:
  0.6 107.2 %shard_map.127 = (bf16[512,768]{1,0:T(8,128)(2,1)}, bf16[512,768]{1,0:T(8,128)(2,1)}, f32[40,768]{1,0:T(8,128)}, f32[16,768]{1,0:T(8,128)}) custom-call(bf16[512,768]{1,0:T(8,128)(2,1)} %cv_hbm.1, bf16[512,768]{1,0:T(8,128)(2,1)} %cg_hbm.1, bf16[512,768]{1,0:T(8,128)(2,1)} %co_hbm.1, bf16[31,768]{1,0:T(8,128)(2,1)} %taps_ref.1, f32[768]{0:T(1024)} %gain_ref.1, ...), custom_call_target="tpu_custom_call" | custom-call | tf_op jit(solution)/shard_map/pallas_call | solution.py:468
  107.8 3.9 %shard_map.128 = (bf16[512,768]{1,0:T(8,128)(2,1)}, bf16[512,768]{1,0:T(8,128)(2,1)}, f32[31,768]{1,0:T(8,128)}, f32[768]{0:T(1024)}, f32[768]{0:T(1024)}, /*index=5*/f32[16,768]{1,0:T(8,128)}) custom-call(bf16[512,768]{1,0:T(8,128)(2,1)} %get-tuple-element.10.gv_in, bf16[512,768]{1,0:T(8,128)(2,1)} %get-tuple-element.11.gg_in, ...), custom_call_target="tpu_custom_call" | custom-call | tf_op jit(solution)/shard_map/pallas_call | solution.py:519
where the time goes:
time: 112 us
  Pallas kernels  111 us (99%)
    pallas_call x1, Pallas kernels, local(): pl.pallas_call(functools.partial(kernel, dims), out_shape=(jax.ShapeDtype...  107 us
    pallas_call x1, Pallas kernels, local(): pl.pallas_call(place, out_shape=(jax.ShapeDtypeStruct((rows, chan), BF16)...  3.87 us

commit v1 on v0

v1 whole, which is shorter than its diff:
```python
import functools
import types

import jax
import jax.numpy as jnp
from jax import lax
from jax.experimental import pallas as pl
from jax.experimental.pallas import tpu as pltpu
from jax.sharding import PartitionSpec as P

norm_eps = 1e-05
MESH = pl.DeviceIdType.MESH
F32 = jnp.float32
BF16 = jnp.bfloat16
LANES = 128
NX, NY, NZ = 4, 4, 8
PLANE = NX * NY
RING = (NX, NY, NZ)
GROUPS = 3
HALO = 32


def repeat(start, stop, body, unroll):
    assert (stop - start) % unroll == 0

    def step(i, carry):
        for u in range(unroll):
            body(start + i * unroll + u)
        return carry

    lax.fori_loop(0, (stop - start) // unroll, step, 0)


def kernel(names, *refs):
    r = types.SimpleNamespace(**dict(zip(names, refs)))
    rows, chan = r.co.shape
    width = r.og.shape[1]
    n = NX * NY * NZ
    block = width // n
    gcols = chan // GROUPS
    cblocks = chan // LANES
    ntaps = r.taps.shape[0]
    reach = ntaps - 1
    per = r.small_out.shape[0]
    share = r.parts.shape[1]
    chan_total = chan * 2
    me = lax.axis_index("sp")
    core = lax.axis_index("tp")
    x = lax.rem(me, NX)
    y = lax.rem(me // NX, NY)
    z = me // PLANE
    spot = lax.rem(me, PLANE)
    axes = ((x, NX, 1), (y, NY, NX), (z, NZ, PLANE))

    def along(axis, delta):
        c, size, stride = axis
        return me + (lax.rem(c + delta, size) - c) * stride

    def in_plane(i):
        return me - spot + lax.rem(spot + i, PLANE)

    def remote(src, dst, send, recv, device, to_core=None):
        return pltpu.make_async_remote_copy(
            src_ref=src, dst_ref=dst, send_sem=send, recv_sem=recv,
            device_id=(device, core if to_core is None else to_core), device_id_type=MESH,
        )

    loads = [
        pltpu.make_async_copy(src, dst, r.in_sem.at[i])
        for i, (src, dst) in enumerate(
            (
                (r.co_hbm, r.co), (r.og_hbm, r.og), (r.w_hbm, r.w), (r.cg_hbm, r.cg), (r.cv_hbm, r.cv),
                (r.taps_hbm, r.taps), (r.gain_hbm, r.gain), (r.shift_hbm, r.shift),
            )
        )
    ]
    loads[0].start()
    barrier = pltpu.get_barrier_semaphore()

    def greet(device, to_core):
        pl.semaphore_signal(barrier, inc=1, device_id=(device, to_core), device_id_type=MESH)

    greet(me, 1 - core)
    for i in range(1, NZ):
        greet(along(axes[2], i), core)
    for i in range(1, PLANE):
        greet(in_plane(i), core)
    has_prev = me > 0
    has_next = me < n - 1

    @pl.when(has_prev)
    def _():
        greet(me - 1, core)

    @pl.when(has_next)
    def _():
        greet(me + 1, core)

    friends = NZ + PLANE - 1 + has_prev.astype(jnp.int32) + has_next.astype(jnp.int32)

    lane_low = lax.broadcasted_iota(jnp.int32, (1, LANES), 1) < LANES // 2
    nt = rows // LANES
    mid = LANES // 2

    def pack(dst):
        for t in range(nt):
            turned = r.st_a[t * LANES:(t + 1) * LANES, :].T
            dst[0, t:t + 1, :] = turned[:1, :]
            dst[1, t:t + 1, :] = turned[mid:mid + 1, :]

    def unpack(packed, dst):
        for t in range(nt):
            dst[t * LANES:(t + 1) * LANES, :] = jnp.broadcast_to(packed[t:t + 1, :], (LANES, LANES)).T

    def wide(v):
        return jnp.concatenate([v] * cblocks, axis=1)

    for copy in loads[1:]:
        copy.start()
    loads[0].wait()

    def stats(i):
        at = pl.ds(pl.multiple_of(i * 64, 64), 64)
        h = r.co[at, :].astype(F32)
        mean = jnp.sum(h, axis=1, keepdims=True) / chan
        d = h - mean
        m2 = jnp.sum(d * d, axis=1, keepdims=True)
        r.st_a[at, :] = jnp.where(lane_low, mean, m2)

    repeat(0, rows // 64, stats, 2)
    pack(r.pk_a)
    pl.semaphore_wait(barrier, friends)
    swap_a = remote(r.pk_a, r.pk_b, r.tp_send.at[0], r.tp_recv.at[0], me, 1 - core)
    swap_a.start()
    loads[1].wait()
    slab = width // NZ

    def transpose(c, carry):
        t = r.og[:, pl.ds(pl.multiple_of(c * slab, slab), slab)].T
        r.ogt[c] = t.reshape(NY, NX, block, rows)
        return carry

    lax.fori_loop(0, NZ, transpose, 0)
    loads[6].wait()
    loads[7].wait()
    gain = r.gain[...].reshape(1, chan)
    shift = r.shift[...].reshape(1, chan)
    swap_a.wait()
    gap = r.pk_a[0] - r.pk_b[0]
    variance = (r.pk_a[1] + r.pk_b[1] + gap * gap * (0.5 * chan)) / chan_total
    unpack(0.5 * (r.pk_a[0] + r.pk_b[0]), r.st_b)
    unpack(lax.rsqrt(variance + norm_eps), r.st_d)

    def norm(i):
        at = pl.ds(pl.multiple_of(i * 32, 32), 32)
        v = (r.co[at, :].astype(F32) - wide(r.st_b[at, :])) * wide(r.st_d[at, :])
        r.normed[at, :] = v
        t = v * gain + shift
        sig = jax.nn.sigmoid(t)
        r.active[at, :] = (t * sig).astype(BF16)
        r.dsilu[at, :] = sig * (1.0 + t * (1.0 - sig))

    repeat(0, rows // 32, norm, 2)

    acc = (r.acc_a, r.acc_b, r.acc_c)
    sent = (r.sent_a, r.sent_b, r.sent_c)
    came = (r.came_a, r.came_b, r.came_c)
    outer = (NZ, NZ, NY)
    second_axis = (1, 0, 0)
    third_axis = (2, 2, 1)

    def hop(g, d, s, k):
        size = RING[g]
        return remote(
            sent[g].at[d, s, k - 1], came[g].at[d, s, k - 1],
            r.ring_send.at[g, d, s, k - 1], r.ring_recv.at[g, d, s, k - 1],
            along(axes[g], 1 if d == 0 else size - 1),
        )

    def product(g, k):
        size = RING[g]
        far = size // 2
        half = outer[g] // 2
        at = lax.rem(axes[g][0] + k, size)
        lhs = r.ogt[:, :, at] if g == 0 else r.ogt[:, at] if g == 1 else r.ogt[at]
        lhs = lhs.reshape(-1, rows)
        out = jnp.dot(lhs, r.active[:, g * gcols:(g + 1) * gcols], preferred_element_type=F32)
        out = out.reshape(outer[g], 4, block, gcols)
        if k == far:
            for d in range(2):
                sent[g][d, d, far - 1] = out[half * d:half * (d + 1)].astype(BF16)
                hop(g, d, d, far).start()
        elif k in (far - 1, size - far + 1):
            d = 0 if k == far - 1 else 1
            s = 1 - d
            sent[g][d, s, far - 2] = out[half * s:half * (s + 1)].astype(BF16)
            hop(g, d, s, far - 1).start()
            acc[g][k, half * d:half * (d + 1)] = out[half * d:half * (d + 1)]
        else:
            acc[g][k] = out

    def relay(g, d, s, k):
        size = RING[g]
        half = outer[g] // 2
        hop(g, d, s, k).wait_recv()
        at = k - 1 if d == 0 else (size - k + 1) % size
        total = acc[g][at, half * s:half * (s + 1)] + came[g][d, s, k - 1].astype(F32)
        if k > 1:
            sent[g][d, s, k - 2] = total.astype(BF16)
            hop(g, d, s, k - 1).start()
        else:
            acc[g][at, half * s:half * (s + 1)] = total

    def second(g, s, i):
        return remote(
            r.sent2.at[g, s, i - 1, pl.ds(0, outer[g] // 2)], r.came2.at[g, s, i - 1, pl.ds(0, outer[g] // 2)],
            r.second_send.at[g, s, i - 1], r.second_recv.at[g, s, i - 1],
            along(axes[second_axis[g]], i),
        )

    def start_second(g, s):
        half = outer[g] // 2
        c = axes[second_axis[g]][0]
        for i in range(1, 4):
            r.sent2[g, s, i - 1, :half] = acc[g][0, half * s:half * (s + 1), lax.rem(c + i, 4)].astype(BF16)
            second(g, s, i).start()

    def finish_second(g, s):
        half = outer[g] // 2
        c = axes[second_axis[g]][0]
        total = acc[g][0, half * s:half * (s + 1), c]
        for i in range(1, 4):
            second(g, s, i).wait_recv()
            total = total + r.came2[g, s, i - 1, :half].astype(F32)
        r.line[g, half * s:half * (s + 1)] = total

    def third(g, i):
        return remote(
            r.sent3.at[g, i - 1], r.came3.at[g, i - 1],
            r.third_send.at[g, i - 1], r.third_recv.at[g, i - 1],
            along(axes[third_axis[g]], i),
        )

    def start_third(g):
        c, size, _ = axes[third_axis[g]]
        for i in range(1, size):
            r.sent3[g, i - 1] = r.line[g, lax.rem(c + i, size)].astype(BF16)
            third(g, i).start()

    def finish_third(g):
        c, size, _ = axes[third_axis[g]]
        total = r.line[g, c]
        for i in range(1, size):
            third(g, i).wait_recv()
            total = total + r.came3[g, i - 1].astype(F32)
        r.proj_out[:, g * gcols:(g + 1) * gcols] = total

    for g, k in ((0, 2), (1, 2), (2, 4)):
        product(g, k)
    for g, k in ((0, 1), (1, 1), (2, 3), (0, 3), (1, 3), (2, 5)):
        product(g, k)
    for g, k in ((2, 2), (2, 6), (2, 1), (2, 7), (0, 0), (1, 0), (2, 0)):
        product(g, k)
    loads[2].wait()
    r.rowacc[...] = jnp.zeros_like(r.rowacc)

    def act(i, carry):
        at = pl.ds(pl.multiple_of(i * 128, 128), 128)
        r.scaled[at, :] = jnp.dot(r.og[at, :], r.w[...], preferred_element_type=F32)
        return carry

    lax.fori_loop(0, rows // 128, act, 0)
    for d in range(2):
        relay(2, d, d, 4)

    def grads(i):
        at = pl.ds(pl.multiple_of(i * 32, 32), 32)
        v = r.normed[at, :]
        ng = r.scaled[at, :] * r.dsilu[at, :]
        ngz = ng * v
        r.rowacc[0] = r.rowacc[0] + jnp.sum(ngz.reshape(4, 8, chan), axis=0)
        r.rowacc[1] = r.rowacc[1] + jnp.sum(ng.reshape(4, 8, chan), axis=0)
        s = ng * gain
        r.scaled[at, :] = s
        total = jnp.sum(s, axis=1, keepdims=True)
        dot = jnp.sum(s * v, axis=1, keepdims=True)
        r.st_a[at, :] = jnp.where(lane_low, total, dot)

    repeat(0, rows // 32, grads, 2)
    pack(r.pk_c)
    swap_b = remote(r.pk_c, r.pk_d, r.tp_send.at[1], r.tp_recv.at[1], me, 1 - core)
    swap_b.start()
    r.tapacc[...] = jnp.zeros_like(r.tapacc)
    loads[5].wait()
    for c in range(cblocks):
        r.tapf[c] = r.taps[:, c * LANES:(c + 1) * LANES].astype(F32)
    r.flat[...] = jnp.zeros_like(r.flat)
    for g in range(2):
        for d in range(2):
            relay(g, d, d, 2)
    for d in range(2):
        relay(2, d, 1 - d, 3)
    swap_b.wait()
    unpack((r.pk_c[0] + r.pk_d[0]) / chan_total, r.st_a)
    unpack((r.pk_c[1] + r.pk_d[1]) / chan_total, r.st_b)

    def height_rows(i):
        at = pl.ds(pl.multiple_of(i * 32, 32), 32)
        hg = wide(r.st_d[at, :]) * (
            r.scaled[at, :] - wide(r.st_a[at, :]) - r.normed[at, :] * wide(r.st_b[at, :])
        )
        for c in range(cblocks):
            r.hgx[c, at, :] = hg[:, c * LANES:(c + 1) * LANES]
        return hg

    first = height_rows(0)
    for c in range(cblocks):
        r.halo_out[c] = first[:, c * LANES:(c + 1) * LANES].astype(BF16)
    halo_copy = remote(r.halo_out, r.halo_in, r.halo_send, r.halo_recv, lax.rem(me + n - 1, n))

    @pl.when(has_prev)
    def _():
        halo_copy.start()

    repeat(1, rows // 32, height_rows, 3)
    loads[3].wait()
    loads[4].wait()
    for d in range(2):
        relay(2, d, d, 3)
    tall = 128
    talls = rows // tall

    def tap_block(c, q):
        at = pl.ds(q, tall)
        cols = pl.ds(pl.multiple_of(c * LANES, LANES), LANES)
        sig = jax.nn.sigmoid(r.cg[at, cols].astype(F32))
        gated = (r.cv[at, cols].astype(F32) * sig).astype(BF16).astype(F32)
        for j in range(ntaps):
            h = r.hgx[c, pl.ds(q + reach - j, tall), :]
            r.tapacc[c, j] = r.tapacc[c, j] + jnp.sum((gated * h).reshape(tall // 8, 8, LANES), axis=0)

    def inner_taps(lo, hi):
        def body(i, carry):
            tap_block(i // (talls - 1), pl.multiple_of(lax.rem(i, talls - 1) * tall, tall))
            return carry

        lax.fori_loop(lo * (talls - 1), hi * (talls - 1), body, 0)

    inner_taps(0, cblocks // 2)
    for d in range(2):
        relay(2, d, 1 - d, 2)
    for g in range(2):
        for d in range(2):
            relay(g, d, 1 - d, 1)
    for d in range(2):
        relay(2, d, d, 2)
    inner_taps(cblocks // 2, cblocks)

    @pl.when(has_next)
    def _():
        halo_copy.wait_recv()
        r.hgx[:, rows:, :] = r.halo_in[...].astype(F32)

    @pl.when(jnp.logical_not(has_next))
    def _():
        r.hgx[:, rows:, :] = jnp.zeros((cblocks, HALO, LANES), F32)


    def last_tap(c, carry):
        tap_block(c, rows - tall)
        return carry

    lax.fori_loop(0, cblocks, last_tap, 0)
    for c in range(cblocks):
        r.flat[c * per:c * per + ntaps, :] = jnp.sum(r.tapacc[c], axis=1)
        for j in range(2):
            r.flat[c * per + ntaps + j:c * per + ntaps + j + 1, :] = jnp.sum(
                r.rowacc[j, :, c * LANES:(c + 1) * LANES], axis=0, keepdims=True
            )

    def piece(ref, i):
        return ref.at[pl.ds(pl.multiple_of(i * share, share), share)]

    def scatter(i):
        return remote(
            piece(r.flat, lax.rem(spot + i, PLANE)), r.parts.at[i - 1],
            r.a_send.at[i - 1], r.a_recv.at[i - 1], in_plane(i),
        )

    def deep(i, sender):
        return remote(
            r.pile.at[z], r.pile.at[sender], r.b_send.at[i - 1], r.b_recv.at[sender], along(axes[2], i),
        )

    def gather(i, sender):
        return remote(
            piece(r.whole, spot), piece(r.whole, sender), r.c_send.at[i - 1], r.c_recv.at[sender], in_plane(i),
        )

    for i in range(1, PLANE):
        scatter(i).start()
    for g in range(2):
        for d in range(2):
            relay(g, d, d, 1)
    for g in range(2):
        for s in range(2):
            start_second(g, s)
    for d in range(2):
        relay(2, d, 1 - d, 1)
    for d in range(2):
        relay(2, d, d, 1)
    for s in range(2):
        start_second(2, s)
    step = 64
    steps = rows // step

    def grad_block(i, carry):
        c = i // steps
        q = pl.multiple_of(lax.rem(i, steps) * step, step)
        at = pl.ds(q, step)
        cols = pl.ds(pl.multiple_of(c * LANES, LANES), LANES)
        sig = jax.nn.sigmoid(r.cg[at, cols].astype(F32))
        value = r.cv[at, cols].astype(F32)
        total = jnp.zeros((step, LANES), F32)
        for j in range(ntaps):
            total = total + r.tapf[c, pl.ds(j, 1), :] * r.hgx[c, pl.ds(q + reach - j, step), :]
        r.gv[at, cols] = (total * sig).astype(BF16)
        r.gg[at, cols] = (total * value * sig * (1.0 - sig)).astype(BF16)
        return carry

    lax.fori_loop(0, 3 * steps, grad_block, 0)
    mine = piece(r.flat, spot)[...]
    for i in range(1, PLANE):
        scatter(i).wait_recv()
        mine = mine + r.parts[i - 1]
    r.pile[z] = mine
    for i in range(1, NZ):
        deep(i, z).start()
    for g in range(2):
        for s in range(2):
            finish_second(g, s)
        start_third(g)
    lax.fori_loop(3 * steps, 5 * steps, grad_block, 0)
    for i in range(1, NZ):
        deep(i, lax.rem(z + i, NZ)).wait_recv()
    mine = r.pile[0]
    for i in range(1, NZ):
        mine = mine + r.pile[i]
    piece(r.whole, spot)[...] = mine
    for i in range(1, PLANE):
        gather(i, spot).start()
    for s in range(2):
        finish_second(2, s)
    start_third(2)
    lax.fori_loop(5 * steps, cblocks * steps, grad_block, 0)
    stores = [
        pltpu.make_async_copy(src, dst, r.out_sem.at[i])
        for i, (src, dst) in enumerate(((r.gv, r.gv_hbm), (r.gg, r.gg_hbm)))
    ]
    for copy in stores:
        copy.start()
    finish_third(0)
    finish_third(1)
    finish_third(2)
    for i in range(1, PLANE):
        gather(i, lax.rem(spot + i, PLANE)).wait_recv()
    for c in range(cblocks):
        r.small_out[:, c * LANES:(c + 1) * LANES] = r.whole[c * per:(c + 1) * per, :]
    for g in range(GROUPS):
        far = RING[g] // 2
        for d in range(2):
            for s in range(2):
                for k in range(1, far + (1 if s == d else 0)):
                    hop(g, d, s, k).wait_send()
        for s in range(2):
            for i in range(1, 4):
                second(g, s, i).wait_send()
        for i in range(1, axes[third_axis[g]][1]):
            third(g, i).wait_send()
    for i in range(1, PLANE):
        scatter(i).wait_send()
        gather(i, spot).wait_send()
    for i in range(1, NZ):
        deep(i, z).wait_send()

    @pl.when(has_prev)
    def _():
        halo_copy.wait_send()

    for copy in stores:
        copy.wait()


def place(gv_in, gg_in, small, proj_in, gv_out, gg_out, taps, gain, shift, proj_out, gv, gg, proj, in_sem, out_sem):
    ins = [
        pltpu.make_async_copy(src, dst, in_sem.at[i])
        for i, (src, dst) in enumerate(((gv_in, gv), (gg_in, gg), (proj_in, proj)))
    ]
    outs = [
        pltpu.make_async_copy(src, dst, out_sem.at[i])
        for i, (src, dst) in enumerate(((gv, gv_out), (gg, gg_out), (proj, proj_out)))
    ]
    for copy in ins:
        copy.start()
    ntaps = taps.shape[0]
    taps[...] = small[:ntaps, :]
    gain[...] = small[ntaps, :]
    shift[...] = small[ntaps + 1, :]
    for came, goes in zip(ins, outs):
        came.wait()
        goes.start()
    for copy in outs:
        copy.wait()


def local(conv_value, conv_gate, conv_out, conv_taps, norm_gain, norm_shift, proj_weight, out_grad):
    rows, chan = conv_value.shape
    ntaps = conv_taps.shape[0]
    width = out_grad.shape[1]
    n = lax.axis_size("sp")
    assert n == NX * NY * NZ and lax.axis_size("tp") == 2
    gcols = chan // GROUPS
    block = width // n
    cblocks = chan // LANES
    per = -(-(ntaps + 2) // 8) * 8
    share = -(-(-(-per * cblocks // PLANE)) // 8) * 8
    hbm = pl.BlockSpec(memory_space=pl.ANY)
    vmem = pl.BlockSpec(memory_space=pltpu.VMEM)
    dma = pltpu.SemaphoreType.DMA

    def ring_buffer(size, deep):
        return pltpu.VMEM((2, 2, size // 2, deep // 2, 4, block, gcols), BF16)

    scratch = dict(
        cv=pltpu.VMEM((rows, chan), BF16),
        cg=pltpu.VMEM((rows, chan), BF16),
        co=pltpu.VMEM((rows, chan), BF16),
        w=pltpu.VMEM((width, chan), BF16),
        og=pltpu.VMEM((rows, width), BF16),
        taps=pltpu.VMEM((ntaps, chan), BF16),
        gain=pltpu.VMEM((chan,), F32),
        shift=pltpu.VMEM((chan,), F32),
        ogt=pltpu.VMEM((NZ, NY, NX, block, rows), BF16),
        active=pltpu.VMEM((rows, chan), BF16),
        normed=pltpu.VMEM((rows, chan), F32),
        dsilu=pltpu.VMEM((rows, chan), F32),
        scaled=pltpu.VMEM((rows, chan), F32),
        hgx=pltpu.VMEM((cblocks, rows + HALO, LANES), F32),
        gv=pltpu.VMEM((rows, chan), BF16),
        gg=pltpu.VMEM((rows, chan), BF16),
        st_a=pltpu.VMEM((rows, LANES), F32),
        st_b=pltpu.VMEM((rows, LANES), F32),
        st_d=pltpu.VMEM((rows, LANES), F32),
        pk_a=pltpu.VMEM((2, rows // LANES, LANES), F32),
        pk_b=pltpu.VMEM((2, rows // LANES, LANES), F32),
        pk_c=pltpu.VMEM((2, rows // LANES, LANES), F32),
        pk_d=pltpu.VMEM((2, rows // LANES, LANES), F32),
        tapf=pltpu.VMEM((cblocks, ntaps, LANES), F32),
        tapacc=pltpu.VMEM((cblocks, ntaps, 8, LANES), F32),
        rowacc=pltpu.VMEM((2, 8, chan), F32),
        halo_out=pltpu.VMEM((cblocks, HALO, LANES), BF16),
        halo_in=pltpu.VMEM((cblocks, HALO, LANES), BF16),
        acc_a=pltpu.VMEM((NX, NZ, 4, block, gcols), F32),
        acc_b=pltpu.VMEM((NY, NZ, 4, block, gcols), F32),
        acc_c=pltpu.VMEM((NZ, NY, 4, block, gcols), F32),
        sent_a=ring_buffer(NX, NZ),
        sent_b=ring_buffer(NY, NZ),
        sent_c=ring_buffer(NZ, NY),
        came_a=ring_buffer(NX, NZ),
        came_b=ring_buffer(NY, NZ),
        came_c=ring_buffer(NZ, NY),
        sent2=pltpu.VMEM((GROUPS, 2, 3, NZ // 2, block, gcols), BF16),
        came2=pltpu.VMEM((GROUPS, 2, 3, NZ // 2, block, gcols), BF16),
        line=pltpu.VMEM((GROUPS, NZ, block, gcols), F32),
        sent3=pltpu.VMEM((GROUPS, NZ - 1, block, gcols), BF16),
        came3=pltpu.VMEM((GROUPS, NZ - 1, block, gcols), BF16),
        flat=pltpu.VMEM((PLANE * share, LANES), F32),
        parts=pltpu.VMEM((PLANE - 1, share, LANES), F32),
        pile=pltpu.VMEM((NZ, share, LANES), F32),
        whole=pltpu.VMEM((PLANE * share, LANES), F32),
        in_sem=dma((8,)),
        out_sem=dma((2,)),
        tp_send=dma((2,)),
        tp_recv=dma((2,)),
        halo_send=dma,
        halo_recv=dma,
        ring_send=dma((GROUPS, 2, 2, NZ // 2)),
        ring_recv=dma((GROUPS, 2, 2, NZ // 2)),
        second_send=dma((GROUPS, 2, 3)),
        second_recv=dma((GROUPS, 2, 3)),
        third_send=dma((GROUPS, NZ - 1)),
        third_recv=dma((GROUPS, NZ - 1)),
        a_send=dma((PLANE - 1,)),
        a_recv=dma((PLANE - 1,)),
        b_send=dma((NZ - 1,)),
        b_recv=dma((NZ,)),
        c_send=dma((PLANE - 1,)),
        c_recv=dma((PLANE,)),
    )
    ins = ("cv_hbm", "cg_hbm", "co_hbm", "taps_hbm", "gain_hbm", "shift_hbm", "w_hbm", "og_hbm")
    outs = ("gv_hbm", "gg_hbm", "small_out", "proj_out")
    grad_value, grad_gate, small, grad_proj = pl.pallas_call(
        functools.partial(kernel, (*ins, *outs, *scratch)),
        out_shape=(
            jax.ShapeDtypeStruct((rows, chan), BF16),
            jax.ShapeDtypeStruct((rows, chan), BF16),
            jax.ShapeDtypeStruct((per, chan), F32),
            jax.ShapeDtypeStruct((block, chan), F32),
        ),
        in_specs=[hbm] * 8,
        out_specs=(hbm, hbm, vmem, vmem),
        scratch_shapes=list(scratch.values()),
        compiler_params=pltpu.CompilerParams(
            collective_id=0, has_side_effects=True, vmem_limit_bytes=60 * 1024 * 1024
        ),
    )(
        conv_value, conv_gate, conv_out, conv_taps, norm_gain, norm_shift, proj_weight, out_grad,
    )
    return pl.pallas_call(
        place,
        out_shape=(
            jax.ShapeDtypeStruct((rows, chan), BF16),
            jax.ShapeDtypeStruct((rows, chan), BF16),
            jax.ShapeDtypeStruct((ntaps, chan), F32),
            jax.ShapeDtypeStruct((chan,), F32),
            jax.ShapeDtypeStruct((chan,), F32),
            jax.ShapeDtypeStruct((block, chan), F32),
        ),
        in_specs=[hbm, hbm, vmem, hbm],
        out_specs=(hbm, hbm, vmem, vmem, vmem, hbm),
        scratch_shapes=[
            pltpu.VMEM((rows, chan), BF16),
            pltpu.VMEM((rows, chan), BF16),
            pltpu.VMEM((block, chan), F32),
            dma((3,)), dma((3,)),
        ],
    )(grad_value, grad_gate, small, grad_proj)


def solution(mesh):
    in_specs = (
        P("sp", "tp"),
        P("sp", "tp"),
        P("sp", "tp"),
        P(None, "tp"),
        P("tp"),
        P("tp"),
        P(None, "tp"),
        P("sp", None),
    )
    out_specs = (P("sp", "tp"), P("sp", "tp"), P(None, "tp"), P("tp"), P("tp"), P("sp", "tp"))
    return jax.shard_map(local, mesh=mesh, in_specs=in_specs, out_specs=out_specs, check_vma=False)
```

time: 112 us -> 52 us (0.46)
  Pallas kernels: 111 us -> 51.2 us
    pallas_call x1, Pallas kernels: 107 us -> 47.3 us  [local(): pl.pallas_call(functools.partial(kernel, (*ins, *outs, *scratch)), out_sh...]
where the time goes in v1:
time: 52 us; the launch traced here: 51.8 us
  Pallas kernels  51.2 us (98%)
  between operations  0.64 us (1%)
    pallas_call x1, Pallas kernels, local(): pl.pallas_call(functools.partial(kernel, (*ins, *outs, *scratch)), out_sh...  47.3 us
    pallas_call x1, Pallas kernels, local(): pl.pallas_call(place, out_shape=(jax.ShapeDtypeStruct((rows, chan), BF16)...  3.87 us

profile of v1, /device:TPU:8, one launch (start us, length us, event | category | flops | bytes accessed | tf_op | source)
XLA Modules:
  0.0 51.8 jit_solution(12512652179843316402)
XLA Ops:
  0.6 47.3 %shard_map.127 = (bf16[512,768]{1,0:T(8,128)(2,1)}, bf16[512,768]{1,0:T(8,128)(2,1)}, f32[40,768]{1,0:T(8,128)}, f32[16,768]{1,0:T(8,128)}) custom-call(bf16[512,768]{1,0:T(8,128)(2,1)} %refs_0_.1, bf16[512,768]{1,0:T(8,128)(2,1)} %refs_1_.1, bf16[512,768]{1,0:T(8,128)(2,1)} %refs_2_.1, bf16[31,768]{1,0:T(8,128)(2,1)} %refs_3_.1, f32[768]{0:T(1024)} %refs_4_.1, ...), custom_call_target="tpu_custom_call" | custom-call | tf_op jit(solution)/shard_map/pallas_call | solution.py:602
  48.0 3.9 %shard_map.128 = (bf16[512,768]{1,0:T(8,128)(2,1)}, bf16[512,768]{1,0:T(8,128)(2,1)}, f32[31,768]{1,0:T(8,128)}, f32[768]{0:T(1024)}, f32[768]{0:T(1024)}, /*index=5*/f32[16,768]{1,0:T(8,128)}) custom-call(bf16[512,768]{1,0:T(8,128)(2,1)} %get-tuple-element.10.gv_in, bf16[512,768]{1,0:T(8,128)(2,1)} %get-tuple-element.11.gg_in, ...), custom_call_target="tpu_custom_call" | custom-call | tf_op jit(solution)/shard_map/pallas_call | solution.py:619

commit v2 on v1

--- a/solution.py
+++ b/solution.py
@@ -18,6 +18,7 @@
 RING = (NX, NY, NZ)
 GROUPS = 3
 HALO = 32
+VMEM_LIMIT = 48 * 1024 * 1024
 
 
 def repeat(start, stop, body, unroll):
@@ -41,7 +42,7 @@
     cblocks = chan // LANES
     ntaps = r.taps.shape[0]
     reach = ntaps - 1
-    per = r.small_out.shape[0]
+    per = -(-(ntaps + 2) // 8) * 8
     share = r.parts.shape[1]
     chan_total = chan * 2
     me = lax.axis_index("sp")
@@ -165,16 +166,24 @@
     acc = (r.acc_a, r.acc_b, r.acc_c)
     sent = (r.sent_a, r.sent_b, r.sent_c)
     came = (r.came_a, r.came_b, r.came_c)
+    sent2 = (r.sent2_a, r.sent2_b, r.sent2_c)
+    came2 = (r.came2_a, r.came2_b, r.came2_c)
+    sent3 = (r.sent3_a, r.sent3_b, r.sent3_c)
+    came3 = (r.came3_a, r.came3_b, r.came3_c)
     outer = (NZ, NZ, NY)
     second_axis = (1, 0, 0)
     third_axis = (2, 2, 1)
+    first_recv = (0, 2 * NX - 2, 2 * NX + 2 * NY - 4)
+
+    def slot(g, d, s, k):
+        far = RING[g] // 2
+        return d * (2 * far - 1) + (k - 1 if s == d else far + k - 1)
 
     def hop(g, d, s, k):
-        size = RING[g]
+        i = slot(g, d, s, k)
         return remote(
-            sent[g].at[d, s, k - 1], came[g].at[d, s, k - 1],
-            r.ring_send.at[g, d, s, k - 1], r.ring_recv.at[g, d, s, k - 1],
-            along(axes[g], 1 if d == 0 else size - 1),
+            sent[g].at[i], came[g].at[i], r.ring_send.at[g], r.ring_recv.at[first_recv[g] + i],
+            along(axes[g], 1 if d == 0 else RING[g] - 1),
         )
 
     def product(g, k):
@@ -188,88 +197,90 @@
         out = out.reshape(outer[g], 4, block, gcols)
         if k == far:
             for d in range(2):
-                sent[g][d, d, far - 1] = out[half * d:half * (d + 1)].astype(BF16)
-                hop(g, d, d, far).start()
+                sent[g][slot(g, d, d, far)] = out[half * d:half * (d + 1)].astype(BF16)
         elif k in (far - 1, size - far + 1):
             d = 0 if k == far - 1 else 1
             s = 1 - d
-            sent[g][d, s, far - 2] = out[half * s:half * (s + 1)].astype(BF16)
-            hop(g, d, s, far - 1).start()
+            sent[g][slot(g, d, s, far - 1)] = out[half * s:half * (s + 1)].astype(BF16)
             acc[g][k, half * d:half * (d + 1)] = out[half * d:half * (d + 1)]
         else:
             acc[g][k] = out
+
+    def launch(g, own):
+        far = RING[g] // 2
+        for d in range(2):
+            if own:
+                hop(g, d, 1 - d, far - 1).start()
+            else:
+                hop(g, d, d, far).start()
 
     def relay(g, d, s, k):
         size = RING[g]
         half = outer[g] // 2
         hop(g, d, s, k).wait_recv()
         at = k - 1 if d == 0 else (size - k + 1) % size
-        total = acc[g][at, half * s:half * (s + 1)] + came[g][d, s, k - 1].astype(F32)
+        total = acc[g][at, half * s:half * (s + 1)] + came[g][slot(g, d, s, k)].astype(F32)
         if k > 1:
-            sent[g][d, s, k - 2] = total.astype(BF16)
+            sent[g][slot(g, d, s, k - 1)] = total.astype(BF16)
             hop(g, d, s, k - 1).start()
         else:
             acc[g][at, half * s:half * (s + 1)] = total
-
-    def second(g, s, i):
-        return remote(
-            r.sent2.at[g, s, i - 1, pl.ds(0, outer[g] // 2)], r.came2.at[g, s, i - 1, pl.ds(0, outer[g] // 2)],
-            r.second_send.at[g, s, i - 1], r.second_recv.at[g, s, i - 1],
-            along(axes[second_axis[g]], i),
-        )
 
     def start_second(g, s):
         half = outer[g] // 2
         c = axes[second_axis[g]][0]
         for i in range(1, 4):
-            r.sent2[g, s, i - 1, :half] = acc[g][0, half * s:half * (s + 1), lax.rem(c + i, 4)].astype(BF16)
-            second(g, s, i).start()
+            sent2[g][s, i - 1] = acc[g][0, half * s:half * (s + 1), lax.rem(c + i, 4)].astype(BF16)
+            remote(
+                sent2[g].at[s, i - 1], came2[g].at[s, i - 1],
+                r.second_send.at[g], r.second_recv.at[g, s], along(axes[second_axis[g]], i),
+            ).start()
 
     def finish_second(g, s):
         half = outer[g] // 2
         c = axes[second_axis[g]][0]
+        remote(sent2[g].at[s], came2[g].at[s], r.second_send.at[g], r.second_recv.at[g, s], me).wait_recv()
         total = acc[g][0, half * s:half * (s + 1), c]
         for i in range(1, 4):
-            second(g, s, i).wait_recv()
-            total = total + r.came2[g, s, i - 1, :half].astype(F32)
+            total = total + came2[g][s, i - 1].astype(F32)
         r.line[g, half * s:half * (s + 1)] = total
-
-    def third(g, i):
-        return remote(
-            r.sent3.at[g, i - 1], r.came3.at[g, i - 1],
-            r.third_send.at[g, i - 1], r.third_recv.at[g, i - 1],
-            along(axes[third_axis[g]], i),
-        )
 
     def start_third(g):
         c, size, _ = axes[third_axis[g]]
         for i in range(1, size):
-            r.sent3[g, i - 1] = r.line[g, lax.rem(c + i, size)].astype(BF16)
-            third(g, i).start()
+            sent3[g][i - 1] = r.line[g, lax.rem(c + i, size)].astype(BF16)
+            remote(
+                sent3[g].at[i - 1], came3[g].at[i - 1],
+                r.third_send.at[g], r.third_recv.at[g], along(axes[third_axis[g]], i),
+            ).start()
 
     def finish_third(g):
         c, size, _ = axes[third_axis[g]]
+        remote(sent3[g], came3[g], r.third_send.at[g], r.third_recv.at[g], me).wait_recv()
         total = r.line[g, c]
         for i in range(1, size):
-            third(g, i).wait_recv()
-            total = total + r.came3[g, i - 1].astype(F32)
+            total = total + came3[g][i - 1].astype(F32)
         r.proj_out[:, g * gcols:(g + 1) * gcols] = total
 
     for g, k in ((0, 2), (1, 2), (2, 4)):
         product(g, k)
-    for g, k in ((0, 1), (1, 1), (2, 3), (0, 3), (1, 3), (2, 5)):
+    for g in range(GROUPS):
+        launch(g, False)
+    for g, k in ((0, 1), (0, 3), (1, 1), (1, 3), (2, 3), (2, 5)):
         product(g, k)
+    for g in range(GROUPS):
+        launch(g, True)
     for g, k in ((2, 2), (2, 6), (2, 1), (2, 7), (0, 0), (1, 0), (2, 0)):
         product(g, k)
     loads[2].wait()
     r.rowacc[...] = jnp.zeros_like(r.rowacc)
 
     def act(i, carry):
-        at = pl.ds(pl.multiple_of(i * 128, 128), 128)
-        r.scaled[at, :] = jnp.dot(r.og[at, :], r.w[...], preferred_element_type=F32)
+        cols = pl.ds(pl.multiple_of(i * gcols, gcols), gcols)
+        r.scaled[:, cols] = jnp.dot(r.og[...], r.w[:, cols], preferred_element_type=F32)
         return carry
 
-    lax.fori_loop(0, rows // 128, act, 0)
+    lax.fori_loop(0, GROUPS, act, 0)
     for d in range(2):
         relay(2, d, d, 4)
 
@@ -325,8 +336,6 @@
     repeat(1, rows // 32, height_rows, 3)
     loads[3].wait()
     loads[4].wait()
-    for d in range(2):
-        relay(2, d, d, 3)
     tall = 128
     talls = rows // tall
 
@@ -348,12 +357,7 @@
 
     inner_taps(0, cblocks // 2)
     for d in range(2):
-        relay(2, d, 1 - d, 2)
-    for g in range(2):
-        for d in range(2):
-            relay(g, d, 1 - d, 1)
-    for d in range(2):
-        relay(2, d, d, 2)
+        relay(2, d, d, 3)
     inner_taps(cblocks // 2, cblocks)
 
     @pl.when(has_next)
@@ -378,39 +382,24 @@
                 r.rowacc[j, :, c * LANES:(c + 1) * LANES], axis=0, keepdims=True
             )
 
-    def piece(ref, i):
-        return ref.at[pl.ds(pl.multiple_of(i * share, share), share)]
-
-    def scatter(i):
-        return remote(
-            piece(r.flat, lax.rem(spot + i, PLANE)), r.parts.at[i - 1],
-            r.a_send.at[i - 1], r.a_recv.at[i - 1], in_plane(i),
-        )
-
-    def deep(i, sender):
-        return remote(
-            r.pile.at[z], r.pile.at[sender], r.b_send.at[i - 1], r.b_recv.at[sender], along(axes[2], i),
-        )
-
-    def gather(i, sender):
-        return remote(
-            piece(r.whole, spot), piece(r.whole, sender), r.c_send.at[i - 1], r.c_recv.at[sender], in_plane(i),
-        )
+    def piece(i):
+        return r.flat.at[pl.ds(pl.multiple_of(i * share, share), share)]
 
     for i in range(1, PLANE):
-        scatter(i).start()
+        remote(
+            piece(lax.rem(spot + i, PLANE)), r.parts.at[i - 1], r.a_send, r.a_recv, in_plane(i),
+        ).start()
+    for g in range(2):
+        for d in range(2):
+            relay(g, d, 1 - d, 1)
+    for d in range(2):
+        relay(2, d, 1 - d, 2)
     for g in range(2):
         for d in range(2):
             relay(g, d, d, 1)
     for g in range(2):
         for s in range(2):
             start_second(g, s)
-    for d in range(2):
-        relay(2, d, 1 - d, 1)
-    for d in range(2):
-        relay(2, d, d, 1)
-    for s in range(2):
-        start_second(2, s)
     step = 64
     steps = rows // step
 
@@ -428,88 +417,81 @@
         r.gg[at, cols] = (total * value * sig * (1.0 - sig)).astype(BF16)
         return carry
 
-    lax.fori_loop(0, 3 * steps, grad_block, 0)
-    mine = piece(r.flat, spot)[...]
+    lax.fori_loop(0, 2 * steps, grad_block, 0)
+    for d in range(2):
+        relay(2, d, d, 2)
+    lax.fori_loop(2 * steps, 4 * steps, grad_block, 0)
+    remote(r.parts, r.parts, r.a_send, r.a_recv, me).wait_recv()
+    mine = piece(spot)[...]
     for i in range(1, PLANE):
-        scatter(i).wait_recv()
         mine = mine + r.parts[i - 1]
-    r.pile[z] = mine
+    r.pile[NZ - 1] = mine
     for i in range(1, NZ):
-        deep(i, z).start()
+        remote(r.pile.at[NZ - 1], r.pile.at[i - 1], r.b_send, r.b_recv, along(axes[2], i)).start()
     for g in range(2):
         for s in range(2):
             finish_second(g, s)
         start_third(g)
-    lax.fori_loop(3 * steps, 5 * steps, grad_block, 0)
+    for d in range(2):
+        relay(2, d, 1 - d, 1)
+    for d in range(2):
+        relay(2, d, d, 1)
+    for s in range(2):
+        start_second(2, s)
+    lax.fori_loop(4 * steps, cblocks * steps, grad_block, 0)
+    nearby = r.pile.at[pl.ds(0, NZ - 1)]
+    remote(nearby, nearby, r.b_send, r.b_recv, me).wait_recv()
+    mine = r.pile[lax.rem(z + NZ - 1, NZ)]
     for i in range(1, NZ):
-        deep(i, lax.rem(z + i, NZ)).wait_recv()
-    mine = r.pile[0]
-    for i in range(1, NZ):
-        mine = mine + r.pile[i]
-    piece(r.whole, spot)[...] = mine
+        mine = mine + r.pile[lax.rem(z - i + 2 * NZ - 1, NZ)]
+    r.whole[PLANE - 1] = mine
     for i in range(1, PLANE):
-        gather(i, spot).start()
+        remote(r.whole.at[PLANE - 1], r.whole.at[i - 1], r.c_send, r.c_recv, in_plane(i)).start()
     for s in range(2):
         finish_second(2, s)
     start_third(2)
-    lax.fori_loop(5 * steps, cblocks * steps, grad_block, 0)
-    stores = [
-        pltpu.make_async_copy(src, dst, r.out_sem.at[i])
-        for i, (src, dst) in enumerate(((r.gv, r.gv_hbm), (r.gg, r.gg_hbm)))
-    ]
-    for copy in stores:
-        copy.start()
     finish_third(0)
     finish_third(1)
+    around = r.whole.at[pl.ds(0, PLANE - 1)]
+    remote(around, around, r.c_send, r.c_recv, me).wait_recv()
+    gains, shifts = [], []
+    for c in range(cblocks):
+        cols = slice(c * LANES, (c + 1) * LANES)
+        for m in range(0, per, 8):
+            row = c * per + m
+            seg = r.whole[lax.rem(spot - row // share + 2 * PLANE - 1, PLANE), row % share:row % share + 8]
+            for q in range(m, m + 8):
+                if q == ntaps:
+                    gains.append(seg[q - m:q - m + 1])
+                elif q == ntaps + 1:
+                    shifts.append(seg[q - m:q - m + 1])
+            if m < ntaps:
+                end = min(m + 8, ntaps)
+                r.taps_out[m:end, cols] = seg[:end - m]
+    r.gain_out[...] = jnp.concatenate(gains, axis=1).reshape(chan)
+    r.shift_out[...] = jnp.concatenate(shifts, axis=1).reshape(chan)
     finish_third(2)
-    for i in range(1, PLANE):
-        gather(i, lax.rem(spot + i, PLANE)).wait_recv()
-    for c in range(cblocks):
-        r.small_out[:, c * LANES:(c + 1) * LANES] = r.whole[c * per:(c + 1) * per, :]
     for g in range(GROUPS):
-        far = RING[g] // 2
-        for d in range(2):
-            for s in range(2):
-                for k in range(1, far + (1 if s == d else 0)):
-                    hop(g, d, s, k).wait_send()
-        for s in range(2):
-            for i in range(1, 4):
-                second(g, s, i).wait_send()
-        for i in range(1, axes[third_axis[g]][1]):
-            third(g, i).wait_send()
-    for i in range(1, PLANE):
-        scatter(i).wait_send()
-        gather(i, spot).wait_send()
-    for i in range(1, NZ):
-        deep(i, z).wait_send()
+        remote(sent[g], came[g], r.ring_send.at[g], r.ring_recv.at[0], me).wait_send()
+        remote(sent2[g], came2[g], r.second_send.at[g], r.second_recv.at[g, 0], me).wait_send()
+        remote(sent3[g], came3[g], r.third_send.at[g], r.third_recv.at[g], me).wait_send()
+    remote(r.parts, r.parts, r.a_send, r.a_recv, me).wait_send()
+    remote(nearby, nearby, r.b_send, r.b_recv, me).wait_send()
+    remote(around, around, r.c_send, r.c_recv, me).wait_send()
 
     @pl.when(has_prev)
     def _():
         halo_copy.wait_send()
 
-    for copy in stores:
-        copy.wait()
-
-
-def place(gv_in, gg_in, small, proj_in, gv_out, gg_out, taps, gain, shift, proj_out, gv, gg, proj, in_sem, out_sem):
-    ins = [
-        pltpu.make_async_copy(src, dst, in_sem.at[i])
-        for i, (src, dst) in enumerate(((gv_in, gv), (gg_in, gg), (proj_in, proj)))
+
+def place(*refs):
+    arrays = (len(refs) - 1) // 2
+    copies = [
+        pltpu.make_async_copy(refs[i], refs[arrays + i], refs[-1].at[i]) for i in range(arrays)
     ]
-    outs = [
-        pltpu.make_async_copy(src, dst, out_sem.at[i])
-        for i, (src, dst) in enumerate(((gv, gv_out), (gg, gg_out), (proj, proj_out)))
-    ]
-    for copy in ins:
+    for copy in copies:
         copy.start()
-    ntaps = taps.shape[0]
-    taps[...] = small[:ntaps, :]
-    gain[...] = small[ntaps, :]
-    shift[...] = small[ntaps + 1, :]
-    for came, goes in zip(ins, outs):
-        came.wait()
-        goes.start()
-    for copy in outs:
+    for copy in copies:
         copy.wait()
 
 
@@ -529,7 +511,10 @@
     dma = pltpu.SemaphoreType.DMA
 
     def ring_buffer(size, deep):
-        return pltpu.VMEM((2, 2, size // 2, deep // 2, 4, block, gcols), BF16)
+        return pltpu.VMEM((2 * size - 2, deep // 2, 4, block, gcols), BF16)
+
+    def pieces(*lead):
+        return pltpu.VMEM((*lead, block, gcols), BF16)
 
     scratch = dict(
         cv=pltpu.VMEM((rows, chan), BF16),
@@ -546,8 +531,6 @@
         dsilu=pltpu.VMEM((rows, chan), F32),
         scaled=pltpu.VMEM((rows, chan), F32),
         hgx=pltpu.VMEM((cblocks, rows + HALO, LANES), F32),
-        gv=pltpu.VMEM((rows, chan), BF16),
-        gg=pltpu.VMEM((rows, chan), BF16),
         st_a=pltpu.VMEM((rows, LANES), F32),
         st_b=pltpu.VMEM((rows, LANES), F32),
         st_d=pltpu.VMEM((rows, LANES), F32),
@@ -569,72 +552,75 @@
         came_a=ring_buffer(NX, NZ),
         came_b=ring_buffer(NY, NZ),
         came_c=ring_buffer(NZ, NY),
-        sent2=pltpu.VMEM((GROUPS, 2, 3, NZ // 2, block, gcols), BF16),
-        came2=pltpu.VMEM((GROUPS, 2, 3, NZ // 2, block, gcols), BF16),
+        sent2_a=pieces(2, 3, NZ // 2),
+        sent2_b=pieces(2, 3, NZ // 2),
+        sent2_c=pieces(2, 3, NY // 2),
+        came2_a=pieces(2, 3, NZ // 2),
+        came2_b=pieces(2, 3, NZ // 2),
+        came2_c=pieces(2, 3, NY // 2),
         line=pltpu.VMEM((GROUPS, NZ, block, gcols), F32),
-        sent3=pltpu.VMEM((GROUPS, NZ - 1, block, gcols), BF16),
-        came3=pltpu.VMEM((GROUPS, NZ - 1, block, gcols), BF16),
+        sent3_a=pieces(NZ - 1),
+        sent3_b=pieces(NZ - 1),
+        sent3_c=pieces(NY - 1),
+        came3_a=pieces(NZ - 1),
+        came3_b=pieces(NZ - 1),
+        came3_c=pieces(NY - 1),
         flat=pltpu.VMEM((PLANE * share, LANES), F32),
         parts=pltpu.VMEM((PLANE - 1, share, LANES), F32),
         pile=pltpu.VMEM((NZ, share, LANES), F32),
-        whole=pltpu.VMEM((PLANE * share, LANES), F32),
+        whole=pltpu.VMEM((PLANE, share, LANES), F32),
         in_sem=dma((8,)),
-        out_sem=dma((2,)),
         tp_send=dma((2,)),
         tp_recv=dma((2,)),
         halo_send=dma,
         halo_recv=dma,
-        ring_send=dma((GROUPS, 2, 2, NZ // 2)),
-        ring_recv=dma((GROUPS, 2, 2, NZ // 2)),
-        second_send=dma((GROUPS, 2, 3)),
-        second_recv=dma((GROUPS, 2, 3)),
-        third_send=dma((GROUPS, NZ - 1)),
-        third_recv=dma((GROUPS, NZ - 1)),
-        a_send=dma((PLANE - 1,)),
-        a_recv=dma((PLANE - 1,)),
-        b_send=dma((NZ - 1,)),
-        b_recv=dma((NZ,)),
-        c_send=dma((PLANE - 1,)),
-        c_recv=dma((PLANE,)),
+        ring_send=dma((GROUPS,)),
+        ring_recv=dma((2 * (NX + NY + NZ) - 6,)),
+        second_send=dma((GROUPS,)),
+        second_recv=dma((GROUPS, 2)),
+        third_send=dma((GROUPS,)),
+        third_recv=dma((GROUPS,)),
+        a_send=dma,
+        a_recv=dma,
+        b_send=dma,
+        b_recv=dma,
+        c_send=dma,
+        c_recv=dma,
     )
     ins = ("cv_hbm", "cg_hbm", "co_hbm", "taps_hbm", "gain_hbm", "shift_hbm", "w_hbm", "og_hbm")
-    outs = ("gv_hbm", "gg_hbm", "small_out", "proj_out")
-    grad_value, grad_gate, small, grad_proj = pl.pallas_call(
+    outs = dict(
+        gv=((rows, chan), BF16),
+        gg=((rows, chan), BF16),
+        taps_out=((ntaps, chan), F32),
+        gain_out=((chan,), F32),
+        shift_out=((chan,), F32),
+        proj_out=((block, chan), F32),
+    )
+    results = pl.pallas_call(
         functools.partial(kernel, (*ins, *outs, *scratch)),
-        out_shape=(
-            jax.ShapeDtypeStruct((rows, chan), BF16),
-            jax.ShapeDtypeStruct((rows, chan), BF16),
-            jax.ShapeDtypeStruct((per, chan), F32),
-            jax.ShapeDtypeStruct((block, chan), F32),
-        ),
-        in_specs=[hbm] * 8,
-        out_specs=(hbm, hbm, vmem, vmem),
+        out_shape=[pltpu.VMEM(*out) for out in outs.values()],
+        in_specs=[pl.BlockSpec(memory_space=pltpu.HBM)] * 8,
+        out_specs=[vmem] * len(outs),
         scratch_shapes=list(scratch.values()),
         compiler_params=pltpu.CompilerParams(
-            collective_id=0, has_side_effects=True, vmem_limit_bytes=60 * 1024 * 1024
+            collective_id=0, has_side_effects=True, vmem_limit_bytes=VMEM_LIMIT
         ),
     )(
-        conv_value, conv_gate, conv_out, conv_taps, norm_gain, norm_shift, proj_weight, out_grad,
+        *[
+            pltpu.with_memory_space_constraint(v, pltpu.HBM)
+            for v in (
+                conv_value, conv_gate, conv_out, conv_taps, norm_gain, norm_shift, proj_weight, out_grad,
+            )
+        ]
     )
     return pl.pallas_call(
         place,
-        out_shape=(
-            jax.ShapeDtypeStruct((rows, chan), BF16),
-            jax.ShapeDtypeStruct((rows, chan), BF16),
-            jax.ShapeDtypeStruct((ntaps, chan), F32),
-            jax.ShapeDtypeStruct((chan,), F32),
-            jax.ShapeDtypeStruct((chan,), F32),
-            jax.ShapeDtypeStruct((block, chan), F32),
-        ),
-        in_specs=[hbm, hbm, vmem, hbm],
-        out_specs=(hbm, hbm, vmem, vmem, vmem, hbm),
-        scratch_shapes=[
-            pltpu.VMEM((rows, chan), BF16),
-            pltpu.VMEM((rows, chan), BF16),
-            pltpu.VMEM((block, chan), F32),
-            dma((3,)), dma((3,)),
-        ],
-    )(grad_value, grad_gate, small, grad_proj)
+        out_shape=[jax.ShapeDtypeStruct(*out) for out in outs.values()],
+        in_specs=[vmem] * len(outs),
+        out_specs=[hbm] * len(outs),
+        scratch_shapes=[dma((len(outs),))],
+        compiler_params=pltpu.CompilerParams(vmem_limit_bytes=1024 * 1024),
+    )(*[pltpu.with_memory_space_constraint(v, pltpu.VMEM) for v in results])
 
 
 def solution(mesh):

time: 52 us -> 43.2 us (0.83); the launches traced: 51.8 us -> 42.4 us
  Pallas kernels: 51.2 us -> 41.8 us
    pallas_call x1, Pallas kernels: 47.3 us -> 40.5 us  [local(): pl.pallas_call(functools.partial(kernel, (*ins, *outs, *scratch)), out_sh...]
    pallas_call x1, Pallas kernels: 3.87 us -> 1.23 us  [local(): pl.pallas_call(place, out_shape=[jax.ShapeDtypeStruct(*out) for out in ou...]
where the time goes in v2:
time: 43.2 us; the launch traced here: 42.4 us
  Pallas kernels  41.8 us (97%)
  between operations  0.64 us (1%)
    pallas_call x1, Pallas kernels, local(): pl.pallas_call(functools.partial(kernel, (*ins, *outs, *scratch)), out_sh...  40.5 us
    pallas_call x1, Pallas kernels, local(): pl.pallas_call(place, out_shape=[jax.ShapeDtypeStruct(*out) for out in ou...  1.23 us

profile of v2, /device:TPU:8, one launch (start us, length us, event | category | flops | bytes accessed | tf_op | source)
XLA Modules:
  0.0 42.4 jit_solution(10742939356851982794)
XLA Ops:
  0.6 40.5 %shard_map.127 = (bf16[512,768]{1,0:T(8,128)(2,1)S(1)}, bf16[512,768]{1,0:T(8,128)(2,1)S(1)}, f32[31,768]{1,0:T(8,128)S(1)}, f32[768]{0:T(1024)S(1)}, f32[768]{0:T(1024)S(1)}, /*index=5*/f32[16,768]{1,0:T(8,128)S(1)}) custom-call(bf16[512,768]{1,0:T(8,128)(2,1)} %refs_0_.1, bf16[512,768]{1,0:T(8,128)(2,1)} %refs_1_.1, bf16[512,768]{1,0:T(8,128)(2,1)} %refs_2_.1, ...), custom_call_target="tpu_custom_call" | custom-call | tf_op jit(solution)/shard_map/pallas_call | solution.py:599
  41.2 1.2 %shard_map.128 = (bf16[512,768]{1,0:T(8,128)(2,1)}, bf16[512,768]{1,0:T(8,128)(2,1)}, f32[31,768]{1,0:T(8,128)}, f32[768]{0:T(1024)}, f32[768]{0:T(1024)}, /*index=5*/f32[16,768]{1,0:T(8,128)}) custom-call(bf16[512,768]{1,0:T(8,128)(2,1)S(1)} %get-tuple-element.12.refs_0_, bf16[512,768]{1,0:T(8,128)(2,1)S(1)} %get-tuple-element.13.refs_1_, ...), custom_call_target="tpu_custom_call" | custom-call | tf_op jit(solution)/shard_map/pallas_call | solution.py:616

commit v3 on v2

--- a/solution.py
+++ b/solution.py
@@ -142,6 +142,21 @@
         return carry
 
     lax.fori_loop(0, NZ, transpose, 0)
+    loads[3].wait()
+    loads[4].wait()
+
+    def gate_rows(i):
+        at = pl.ds(pl.multiple_of(i * 32, 32), 32)
+        value = r.cv[at, :].astype(F32)
+        return (value * jax.nn.sigmoid(r.cg[at, :].astype(F32))).astype(BF16)
+
+    r.gate_out[...] = gate_rows(rows // HALO - 1)
+    gate_copy = remote(r.gate_out, r.gate_in, r.gate_send, r.gate_recv, lax.rem(me + 1, n))
+
+    @pl.when(has_next)
+    def _():
+        gate_copy.start()
+
     loads[6].wait()
     loads[7].wait()
     gain = r.gain[...].reshape(1, chan)
@@ -166,13 +181,13 @@
     acc = (r.acc_a, r.acc_b, r.acc_c)
     sent = (r.sent_a, r.sent_b, r.sent_c)
     came = (r.came_a, r.came_b, r.came_c)
-    sent2 = (r.sent2_a, r.sent2_b, r.sent2_c)
-    came2 = (r.came2_a, r.came2_b, r.came2_c)
-    sent3 = (r.sent3_a, r.sent3_b, r.sent3_c)
-    came3 = (r.came3_a, r.came3_b, r.came3_c)
+    sent2 = (r.sent2_a, r.sent2_b)
+    came2 = (r.came2_a, r.came2_b)
+    sent3 = (r.sent3_a, r.sent3_b)
+    came3 = (r.came3_a, r.came3_b)
     outer = (NZ, NZ, NY)
-    second_axis = (1, 0, 0)
-    third_axis = (2, 2, 1)
+    second_axis = (1, 0)
+    third_axis = (2, 2)
     first_recv = (0, 2 * NX - 2, 2 * NX + 2 * NY - 4)
 
     def slot(g, d, s, k):
@@ -226,6 +241,19 @@
         else:
             acc[g][at, half * s:half * (s + 1)] = total
 
+    def start_plane():
+        for i in range(1, PLANE):
+            peer = lax.rem(spot + i, PLANE)
+            r.sent_p[i - 1] = acc[2][0, peer // NX, lax.rem(peer, NX)].astype(BF16)
+            remote(r.sent_p.at[i - 1], r.came_p.at[i - 1], r.plane_send, r.plane_recv, in_plane(i)).start()
+
+    def finish_plane():
+        remote(r.sent_p, r.came_p, r.plane_send, r.plane_recv, me).wait_recv()
+        total = acc[2][0, y, x]
+        for i in range(1, PLANE):
+            total = total + r.came_p[i - 1].astype(F32)
+        r.proj_out[:, 2 * gcols:] = total
+
     def start_second(g, s):
         half = outer[g] // 2
         c = axes[second_axis[g]][0]
@@ -262,42 +290,52 @@
             total = total + came3[g][i - 1].astype(F32)
         r.proj_out[:, g * gcols:(g + 1) * gcols] = total
 
-    for g, k in ((0, 2), (1, 2), (2, 4)):
+    for g, k in ((2, 4), (0, 2), (1, 2)):
         product(g, k)
-    for g in range(GROUPS):
+    for g in (2, 0, 1):
         launch(g, False)
-    for g, k in ((0, 1), (0, 3), (1, 1), (1, 3), (2, 3), (2, 5)):
+    for g, k in ((2, 3), (2, 5), (0, 1), (0, 3), (1, 1), (1, 3)):
         product(g, k)
-    for g in range(GROUPS):
+    for g in (2, 0, 1):
         launch(g, True)
-    for g, k in ((2, 2), (2, 6), (2, 1), (2, 7), (0, 0), (1, 0), (2, 0)):
-        product(g, k)
     loads[2].wait()
-    r.rowacc[...] = jnp.zeros_like(r.rowacc)
-
-    def act(i, carry):
-        cols = pl.ds(pl.multiple_of(i * gcols, gcols), gcols)
+
+    def act(i):
+        cols = slice(i * gcols, (i + 1) * gcols)
         r.scaled[:, cols] = jnp.dot(r.og[...], r.w[:, cols], preferred_element_type=F32)
-        return carry
-
-    lax.fori_loop(0, GROUPS, act, 0)
-    for d in range(2):
-        relay(2, d, d, 4)
 
     def grads(i):
-        at = pl.ds(pl.multiple_of(i * 32, 32), 32)
-        v = r.normed[at, :]
-        ng = r.scaled[at, :] * r.dsilu[at, :]
-        ngz = ng * v
-        r.rowacc[0] = r.rowacc[0] + jnp.sum(ngz.reshape(4, 8, chan), axis=0)
-        r.rowacc[1] = r.rowacc[1] + jnp.sum(ng.reshape(4, 8, chan), axis=0)
-        s = ng * gain
-        r.scaled[at, :] = s
-        total = jnp.sum(s, axis=1, keepdims=True)
-        dot = jnp.sum(s * v, axis=1, keepdims=True)
+        cols = slice(i * gcols, (i + 1) * gcols)
+        sums = [jnp.zeros((8, gcols), F32)] * 2
+        for q in range(0, rows, 32):
+            at = slice(q, q + 32)
+            v = r.normed[at, cols]
+            ng = r.scaled[at, cols] * r.dsilu[at, cols]
+            sums = [
+                sums[0] + jnp.sum((ng * v).reshape(4, 8, gcols), axis=0),
+                sums[1] + jnp.sum(ng.reshape(4, 8, gcols), axis=0),
+            ]
+            s = ng * gain[:, cols]
+            r.scaled[at, cols] = s
+            for dst, t in ((r.st_a, s), (r.st_b, s * v)):
+                t = t[:, :LANES] + t[:, LANES:]
+                dst[at, :] = t if i == 0 else dst[at, :] + t
+        for j in range(2):
+            r.rowacc[j, :, cols] = sums[j]
+
+    act(0)
+    for i in range(1, GROUPS):
+        act(i)
+        grads(i - 1)
+    grads(GROUPS - 1)
+
+    def fold(i):
+        at = pl.ds(pl.multiple_of(i * 64, 64), 64)
+        total = jnp.sum(r.st_a[at, :], axis=1, keepdims=True)
+        dot = jnp.sum(r.st_b[at, :], axis=1, keepdims=True)
         r.st_a[at, :] = jnp.where(lane_low, total, dot)
 
-    repeat(0, rows // 32, grads, 2)
+    repeat(0, rows // 64, fold, 2)
     pack(r.pk_c)
     swap_b = remote(r.pk_c, r.pk_d, r.tp_send.at[1], r.tp_recv.at[1], me, 1 - core)
     swap_b.start()
@@ -306,11 +344,29 @@
     for c in range(cblocks):
         r.tapf[c] = r.taps[:, c * LANES:(c + 1) * LANES].astype(F32)
     r.flat[...] = jnp.zeros_like(r.flat)
-    for g in range(2):
-        for d in range(2):
-            relay(g, d, d, 2)
     for d in range(2):
-        relay(2, d, 1 - d, 3)
+        relay(2, d, d, 4)
+
+    def gate(i):
+        at = pl.ds(pl.multiple_of(HALO + i * 32, 32), 32)
+        gated = gate_rows(i).astype(F32)
+        for c in range(cblocks):
+            r.gx[c, at, :] = gated[:, c * LANES:(c + 1) * LANES]
+
+    repeat(0, rows // 32, gate, 2)
+
+    @pl.when(has_prev)
+    def _():
+        gate_copy.wait_recv()
+        for c in range(cblocks):
+            r.gx[c, :HALO, :] = r.gate_in[:, c * LANES:(c + 1) * LANES].astype(F32)
+
+    @pl.when(jnp.logical_not(has_prev))
+    def _():
+        r.gx[:, :HALO, :] = jnp.zeros((cblocks, HALO, LANES), F32)
+
+    for k in (2, 6):
+        product(2, k)
     swap_b.wait()
     unpack((r.pk_c[0] + r.pk_d[0]) / chan_total, r.st_a)
     unpack((r.pk_c[1] + r.pk_d[1]) / chan_total, r.st_b)
@@ -334,47 +390,32 @@
         halo_copy.start()
 
     repeat(1, rows // 32, height_rows, 3)
-    loads[3].wait()
-    loads[4].wait()
+    for g in range(2):
+        for d in range(2):
+            relay(g, d, d, 2)
+    for d in range(2):
+        relay(2, d, 1 - d, 3)
     tall = 128
     talls = rows // tall
-
-    def tap_block(c, q):
-        at = pl.ds(q, tall)
-        cols = pl.ds(pl.multiple_of(c * LANES, LANES), LANES)
-        sig = jax.nn.sigmoid(r.cg[at, cols].astype(F32))
-        gated = (r.cv[at, cols].astype(F32) * sig).astype(BF16).astype(F32)
-        for j in range(ntaps):
-            h = r.hgx[c, pl.ds(q + reach - j, tall), :]
-            r.tapacc[c, j] = r.tapacc[c, j] + jnp.sum((gated * h).reshape(tall // 8, 8, LANES), axis=0)
-
-    def inner_taps(lo, hi):
-        def body(i, carry):
-            tap_block(i // (talls - 1), pl.multiple_of(lax.rem(i, talls - 1) * tall, tall))
-            return carry
-
-        lax.fori_loop(lo * (talls - 1), hi * (talls - 1), body, 0)
-
-    inner_taps(0, cblocks // 2)
+    skip = HALO - reach
+
+    def tap_block(i, carry):
+        c = i // talls
+        q = pl.multiple_of(lax.rem(i, talls) * tall, tall)
+        hg = r.hgx[c, pl.ds(q, tall), :]
+        for m in range(8):
+            js = range(m, ntaps, 8)
+            near = r.gx[c, pl.ds(q + skip + m, tall + 8 * (len(js) - 1)), :]
+            for k, j in enumerate(js):
+                both = near[8 * k:8 * k + tall] * hg
+                r.tapacc[c, j] = r.tapacc[c, j] + jnp.sum(both.reshape(tall // 8, 8, LANES), axis=0)
+        return carry
+
+    early = 16
+    lax.fori_loop(0, early, tap_block, 0)
     for d in range(2):
         relay(2, d, d, 3)
-    inner_taps(cblocks // 2, cblocks)
-
-    @pl.when(has_next)
-    def _():
-        halo_copy.wait_recv()
-        r.hgx[:, rows:, :] = r.halo_in[...].astype(F32)
-
-    @pl.when(jnp.logical_not(has_next))
-    def _():
-        r.hgx[:, rows:, :] = jnp.zeros((cblocks, HALO, LANES), F32)
-
-
-    def last_tap(c, carry):
-        tap_block(c, rows - tall)
-        return carry
-
-    lax.fori_loop(0, cblocks, last_tap, 0)
+    lax.fori_loop(early, cblocks * talls, tap_block, 0)
     for c in range(cblocks):
         r.flat[c * per:c * per + ntaps, :] = jnp.sum(r.tapacc[c], axis=1)
         for j in range(2):
@@ -389,11 +430,11 @@
         remote(
             piece(lax.rem(spot + i, PLANE)), r.parts.at[i - 1], r.a_send, r.a_recv, in_plane(i),
         ).start()
+    for g, k in ((0, 0), (1, 0), (2, 1), (2, 7), (2, 0)):
+        product(g, k)
     for g in range(2):
         for d in range(2):
             relay(g, d, 1 - d, 1)
-    for d in range(2):
-        relay(2, d, 1 - d, 2)
     for g in range(2):
         for d in range(2):
             relay(g, d, d, 1)
@@ -404,23 +445,29 @@
     steps = rows // step
 
     def grad_block(i, carry):
-        c = i // steps
-        q = pl.multiple_of(lax.rem(i, steps) * step, step)
+        inner = i < cblocks * (steps - 1)
+        c = jnp.where(inner, i // (steps - 1), i - cblocks * (steps - 1))
+        q = pl.multiple_of(jnp.where(inner, lax.rem(i, steps - 1), steps - 1) * step, step)
         at = pl.ds(q, step)
         cols = pl.ds(pl.multiple_of(c * LANES, LANES), LANES)
         sig = jax.nn.sigmoid(r.cg[at, cols].astype(F32))
         value = r.cv[at, cols].astype(F32)
         total = jnp.zeros((step, LANES), F32)
-        for j in range(ntaps):
-            total = total + r.tapf[c, pl.ds(j, 1), :] * r.hgx[c, pl.ds(q + reach - j, step), :]
+        for m in range(8):
+            ks = range(m, ntaps, 8)
+            near = r.hgx[c, pl.ds(q + m, step + 8 * (len(ks) - 1)), :]
+            for k, j in enumerate(ks):
+                total = total + r.tapf[c, pl.ds(reach - j, 1), :] * near[8 * k:8 * k + step]
         r.gv[at, cols] = (total * sig).astype(BF16)
         r.gg[at, cols] = (total * value * sig * (1.0 - sig)).astype(BF16)
         return carry
 
-    lax.fori_loop(0, 2 * steps, grad_block, 0)
+    lax.fori_loop(0, 7, grad_block, 0)
+    for d in range(2):
+        relay(2, d, 1 - d, 2)
     for d in range(2):
         relay(2, d, d, 2)
-    lax.fori_loop(2 * steps, 4 * steps, grad_block, 0)
+    lax.fori_loop(7, 28, grad_block, 0)
     remote(r.parts, r.parts, r.a_send, r.a_recv, me).wait_recv()
     mine = piece(spot)[...]
     for i in range(1, PLANE):
@@ -428,28 +475,35 @@
     r.pile[NZ - 1] = mine
     for i in range(1, NZ):
         remote(r.pile.at[NZ - 1], r.pile.at[i - 1], r.b_send, r.b_recv, along(axes[2], i)).start()
+    lax.fori_loop(28, 36, grad_block, 0)
+    for d in range(2):
+        relay(2, d, 1 - d, 1)
+    for d in range(2):
+        relay(2, d, d, 1)
+    start_plane()
     for g in range(2):
         for s in range(2):
             finish_second(g, s)
         start_third(g)
-    for d in range(2):
-        relay(2, d, 1 - d, 1)
-    for d in range(2):
-        relay(2, d, d, 1)
-    for s in range(2):
-        start_second(2, s)
-    lax.fori_loop(4 * steps, cblocks * steps, grad_block, 0)
+
+    @pl.when(has_next)
+    def _():
+        halo_copy.wait_recv()
+        r.hgx[:, rows:, :] = r.halo_in[...].astype(F32)
+
+    @pl.when(jnp.logical_not(has_next))
+    def _():
+        r.hgx[:, rows:, :] = jnp.zeros((cblocks, HALO, LANES), F32)
+
+    lax.fori_loop(36, cblocks * steps, grad_block, 0)
     nearby = r.pile.at[pl.ds(0, NZ - 1)]
     remote(nearby, nearby, r.b_send, r.b_recv, me).wait_recv()
     mine = r.pile[lax.rem(z + NZ - 1, NZ)]
     for i in range(1, NZ):
         mine = mine + r.pile[lax.rem(z - i + 2 * NZ - 1, NZ)]
-    r.whole[PLANE - 1] = mine
+    r.whole[PLANE - 1] = mine.astype(BF16)
     for i in range(1, PLANE):
         remote(r.whole.at[PLANE - 1], r.whole.at[i - 1], r.c_send, r.c_recv, in_plane(i)).start()
-    for s in range(2):
-        finish_second(2, s)
-    start_third(2)
     finish_third(0)
     finish_third(1)
     around = r.whole.at[pl.ds(0, PLANE - 1)]
@@ -459,7 +513,8 @@
         cols = slice(c * LANES, (c + 1) * LANES)
         for m in range(0, per, 8):
             row = c * per + m
-            seg = r.whole[lax.rem(spot - row // share + 2 * PLANE - 1, PLANE), row % share:row % share + 8]
+            seg = r.whole[lax.rem(spot - row // share + 2 * PLANE - 1, PLANE)].astype(F32)
+            seg = seg[row % share:row % share + 8]
             for q in range(m, m + 8):
                 if q == ntaps:
                     gains.append(seg[q - m:q - m + 1])
@@ -470,11 +525,13 @@
                 r.taps_out[m:end, cols] = seg[:end - m]
     r.gain_out[...] = jnp.concatenate(gains, axis=1).reshape(chan)
     r.shift_out[...] = jnp.concatenate(shifts, axis=1).reshape(chan)
-    finish_third(2)
+    finish_plane()
     for g in range(GROUPS):
         remote(sent[g], came[g], r.ring_send.at[g], r.ring_recv.at[0], me).wait_send()
+    for g in range(2):
         remote(sent2[g], came2[g], r.second_send.at[g], r.second_recv.at[g, 0], me).wait_send()
         remote(sent3[g], came3[g], r.third_send.at[g], r.third_recv.at[g], me).wait_send()
+    remote(r.sent_p, r.came_p, r.plane_send, r.plane_recv, me).wait_send()
     remote(r.parts, r.parts, r.a_send, r.a_recv, me).wait_send()
     remote(nearby, nearby, r.b_send, r.b_recv, me).wait_send()
     remote(around, around, r.c_send, r.c_recv, me).wait_send()
@@ -482,6 +539,10 @@
     @pl.when(has_prev)
     def _():
         halo_copy.wait_send()
+
+    @pl.when(has_next)
+    def _():
+        gate_copy.wait_send()
 
 
 def place(*refs):
@@ -541,6 +602,9 @@
         tapf=pltpu.VMEM((cblocks, ntaps, LANES), F32),
         tapacc=pltpu.VMEM((cblocks, ntaps, 8, LANES), F32),
         rowacc=pltpu.VMEM((2, 8, chan), F32),
+        gx=pltpu.VMEM((cblocks, HALO + rows, LANES), F32),
+        gate_out=pltpu.VMEM((HALO, chan), BF16),
+        gate_in=pltpu.VMEM((HALO, chan), BF16),
         halo_out=pltpu.VMEM((cblocks, HALO, LANES), BF16),
         halo_in=pltpu.VMEM((cblocks, HALO, LANES), BF16),
         acc_a=pltpu.VMEM((NX, NZ, 4, block, gcols), F32),
@@ -554,21 +618,19 @@
         came_c=ring_buffer(NZ, NY),
         sent2_a=pieces(2, 3, NZ // 2),
         sent2_b=pieces(2, 3, NZ // 2),
-        sent2_c=pieces(2, 3, NY // 2),
         came2_a=pieces(2, 3, NZ // 2),
         came2_b=pieces(2, 3, NZ // 2),
-        came2_c=pieces(2, 3, NY // 2),
-        line=pltpu.VMEM((GROUPS, NZ, block, gcols), F32),
+        line=pltpu.VMEM((2, NZ, block, gcols), F32),
         sent3_a=pieces(NZ - 1),
         sent3_b=pieces(NZ - 1),
-        sent3_c=pieces(NY - 1),
         came3_a=pieces(NZ - 1),
         came3_b=pieces(NZ - 1),
-        came3_c=pieces(NY - 1),
+        sent_p=pieces(PLANE - 1),
+        came_p=pieces(PLANE - 1),
         flat=pltpu.VMEM((PLANE * share, LANES), F32),
         parts=pltpu.VMEM((PLANE - 1, share, LANES), F32),
         pile=pltpu.VMEM((NZ, share, LANES), F32),
-        whole=pltpu.VMEM((PLANE, share, LANES), F32),
+        whole=pltpu.VMEM((PLANE, share, LANES), BF16),
         in_sem=dma((8,)),
         tp_send=dma((2,)),
         tp_recv=dma((2,)),
@@ -576,10 +638,14 @@
         halo_recv=dma,
         ring_send=dma((GROUPS,)),
         ring_recv=dma((2 * (NX + NY + NZ) - 6,)),
-        second_send=dma((GROUPS,)),
-        second_recv=dma((GROUPS, 2)),
-        third_send=dma((GROUPS,)),
-        third_recv=dma((GROUPS,)),
+        second_send=dma((2,)),
+        second_recv=dma((2, 2)),
+        third_send=dma((2,)),
+        third_recv=dma((2,)),
+        plane_send=dma,
+        plane_recv=dma,
+        gate_send=dma,
+        gate_recv=dma,
         a_send=dma,
         a_recv=dma,
         b_send=dma,

time: 43.2 us -> 39.8 us (0.921); the launches traced: 42.4 us -> 39.7 us
  Pallas kernels: 41.8 us -> 39.1 us
    pallas_call x1, Pallas kernels: 40.5 us -> 37.9 us  [local(): pl.pallas_call(functools.partial(kernel, (*ins, *outs, *scratch)), out_sh...]
where the time goes in v3:
time: 39.8 us; the launch traced here: 39.7 us
  Pallas kernels  39.1 us (98%)
  between operations  0.64 us (2%)
    pallas_call x1, Pallas kernels, local(): pl.pallas_call(functools.partial(kernel, (*ins, *outs, *scratch)), out_sh...  37.9 us
    pallas_call x1, Pallas kernels, local(): pl.pallas_call(place, out_shape=[jax.ShapeDtypeStruct(*out) for out in ou...  1.23 us

profile of v3, /device:TPU:8, one launch (start us, length us, event | category | flops | bytes accessed | tf_op | source)
XLA Modules:
  0.0 39.7 jit_solution(535126136898554239)
XLA Ops:
  0.6 37.9 %shard_map.127 = (bf16[512,768]{1,0:T(8,128)(2,1)S(1)}, bf16[512,768]{1,0:T(8,128)(2,1)S(1)}, f32[31,768]{1,0:T(8,128)S(1)}, f32[768]{0:T(1024)S(1)}, f32[768]{0:T(1024)S(1)}, /*index=5*/f32[16,768]{1,0:T(8,128)S(1)}) custom-call(bf16[512,768]{1,0:T(8,128)(2,1)} %refs_0_.1, bf16[512,768]{1,0:T(8,128)(2,1)} %refs_1_.1, bf16[512,768]{1,0:T(8,128)(2,1)} %refs_2_.1, ...), custom_call_target="tpu_custom_call" | custom-call | tf_op jit(solution)/shard_map/pallas_call | solution.py:665
  38.5 1.2 %shard_map.128 = (bf16[512,768]{1,0:T(8,128)(2,1)}, bf16[512,768]{1,0:T(8,128)(2,1)}, f32[31,768]{1,0:T(8,128)}, f32[768]{0:T(1024)}, f32[768]{0:T(1024)}, /*index=5*/f32[16,768]{1,0:T(8,128)}) custom-call(bf16[512,768]{1,0:T(8,128)(2,1)S(1)} %get-tuple-element.12.refs_0_, bf16[512,768]{1,0:T(8,128)(2,1)S(1)} %get-tuple-element.13.refs_1_, ...), custom_call_target="tpu_custom_call" | custom-call | tf_op jit(solution)/shard_map/pallas_call | solution.py:682

commit v4 on v3

--- a/solution.py
+++ b/solution.py
@@ -43,7 +43,7 @@
     ntaps = r.taps.shape[0]
     reach = ntaps - 1
     per = -(-(ntaps + 2) // 8) * 8
-    share = r.parts.shape[1]
+    share = r.parts.shape[2]
     chan_total = chan * 2
     me = lax.axis_index("sp")
     core = lax.axis_index("tp")
@@ -86,6 +86,7 @@
         greet(along(axes[2], i), core)
     for i in range(1, PLANE):
         greet(in_plane(i), core)
+        greet(in_plane(i), 1 - core)
     has_prev = me > 0
     has_next = me < n - 1
 
@@ -97,7 +98,7 @@
     def _():
         greet(me + 1, core)
 
-    friends = NZ + PLANE - 1 + has_prev.astype(jnp.int32) + has_next.astype(jnp.int32)
+    friends = NZ + 2 * (PLANE - 1) + has_prev.astype(jnp.int32) + has_next.astype(jnp.int32)
 
     lane_low = lax.broadcasted_iota(jnp.int32, (1, LANES), 1) < LANES // 2
     nt = rows // LANES
@@ -116,20 +117,48 @@
     def wide(v):
         return jnp.concatenate([v] * cblocks, axis=1)
 
-    for copy in loads[1:]:
-        copy.start()
+    for i in (3, 4, 1, 2, 6, 7, 5):
+        loads[i].start()
     loads[0].wait()
 
-    def stats(i):
-        at = pl.ds(pl.multiple_of(i * 64, 64), 64)
+    def means(i):
+        at = slice(i * 64, (i + 1) * 64)
         h = r.co[at, :].astype(F32)
         mean = jnp.sum(h, axis=1, keepdims=True) / chan
-        d = h - mean
-        m2 = jnp.sum(d * d, axis=1, keepdims=True)
-        r.st_a[at, :] = jnp.where(lane_low, mean, m2)
-
-    repeat(0, rows // 64, stats, 2)
+        r.st_b[at, :] = jnp.broadcast_to(mean, (64, LANES))
+
+    def spreads(i):
+        at = slice(i * 64, (i + 1) * 64)
+        mean = r.st_b[at, :]
+        m2 = jnp.zeros((64, LANES), F32)
+        for c in range(cblocks):
+            d = r.co[at, c * LANES:(c + 1) * LANES].astype(F32) - mean
+            m2 = m2 + d * d
+        r.st_a[at, :] = jnp.where(lane_low, mean, jnp.sum(m2, axis=1, keepdims=True))
+
+    for i in range(rows // 64):
+        means(i)
+    for i in range(rows // 64):
+        spreads(i)
     pack(r.pk_a)
+    loads[3].wait()
+    loads[4].wait()
+
+    def gate_rows(i):
+        at = pl.ds(pl.multiple_of(i * 32, 32), 32)
+        value = r.cv[at, :].astype(F32)
+        return (value * jax.nn.sigmoid(r.cg[at, :].astype(F32))).astype(BF16)
+
+    r.gate_out[...] = gate_rows(rows // HALO - 1)
+
+    def gate(i):
+        at = pl.ds(pl.multiple_of(HALO + i * 32, 32), 32)
+        gated = gate_rows(i).astype(F32)
+        for c in range(cblocks):
+            r.gx[c, at, :] = gated[:, c * LANES:(c + 1) * LANES]
+
+    repeat(0, rows // 32, gate, 2)
+
     pl.semaphore_wait(barrier, friends)
     swap_a = remote(r.pk_a, r.pk_b, r.tp_send.at[0], r.tp_recv.at[0], me, 1 - core)
     swap_a.start()
@@ -142,15 +171,6 @@
         return carry
 
     lax.fori_loop(0, NZ, transpose, 0)
-    loads[3].wait()
-    loads[4].wait()
-
-    def gate_rows(i):
-        at = pl.ds(pl.multiple_of(i * 32, 32), 32)
-        value = r.cv[at, :].astype(F32)
-        return (value * jax.nn.sigmoid(r.cg[at, :].astype(F32))).astype(BF16)
-
-    r.gate_out[...] = gate_rows(rows // HALO - 1)
     gate_copy = remote(r.gate_out, r.gate_in, r.gate_send, r.gate_recv, lax.rem(me + 1, n))
 
     @pl.when(has_next)
@@ -168,7 +188,7 @@
     unpack(lax.rsqrt(variance + norm_eps), r.st_d)
 
     def norm(i):
-        at = pl.ds(pl.multiple_of(i * 32, 32), 32)
+        at = pl.ds(pl.multiple_of(i * 16, 16), 16)
         v = (r.co[at, :].astype(F32) - wide(r.st_b[at, :])) * wide(r.st_d[at, :])
         r.normed[at, :] = v
         t = v * gain + shift
@@ -176,7 +196,7 @@
         r.active[at, :] = (t * sig).astype(BF16)
         r.dsilu[at, :] = sig * (1.0 + t * (1.0 - sig))
 
-    repeat(0, rows // 32, norm, 2)
+    repeat(0, rows // 16, norm, 4)
 
     acc = (r.acc_a, r.acc_b, r.acc_c)
     sent = (r.sent_a, r.sent_b, r.sent_c)
@@ -329,13 +349,12 @@
         grads(i - 1)
     grads(GROUPS - 1)
 
-    def fold(i):
-        at = pl.ds(pl.multiple_of(i * 64, 64), 64)
+    for q in range(0, rows, 64):
+        at = slice(q, q + 64)
         total = jnp.sum(r.st_a[at, :], axis=1, keepdims=True)
         dot = jnp.sum(r.st_b[at, :], axis=1, keepdims=True)
         r.st_a[at, :] = jnp.where(lane_low, total, dot)
 
-    repeat(0, rows // 64, fold, 2)
     pack(r.pk_c)
     swap_b = remote(r.pk_c, r.pk_d, r.tp_send.at[1], r.tp_recv.at[1], me, 1 - core)
     swap_b.start()
@@ -344,29 +363,10 @@
     for c in range(cblocks):
         r.tapf[c] = r.taps[:, c * LANES:(c + 1) * LANES].astype(F32)
     r.flat[...] = jnp.zeros_like(r.flat)
+    for g, k in ((2, 2), (2, 6), (0, 0), (1, 0)):
+        product(g, k)
     for d in range(2):
         relay(2, d, d, 4)
-
-    def gate(i):
-        at = pl.ds(pl.multiple_of(HALO + i * 32, 32), 32)
-        gated = gate_rows(i).astype(F32)
-        for c in range(cblocks):
-            r.gx[c, at, :] = gated[:, c * LANES:(c + 1) * LANES]
-
-    repeat(0, rows // 32, gate, 2)
-
-    @pl.when(has_prev)
-    def _():
-        gate_copy.wait_recv()
-        for c in range(cblocks):
-            r.gx[c, :HALO, :] = r.gate_in[:, c * LANES:(c + 1) * LANES].astype(F32)
-
-    @pl.when(jnp.logical_not(has_prev))
-    def _():
-        r.gx[:, :HALO, :] = jnp.zeros((cblocks, HALO, LANES), F32)
-
-    for k in (2, 6):
-        product(2, k)
     swap_b.wait()
     unpack((r.pk_c[0] + r.pk_d[0]) / chan_total, r.st_a)
     unpack((r.pk_c[1] + r.pk_d[1]) / chan_total, r.st_b)
@@ -390,11 +390,16 @@
         halo_copy.start()
 
     repeat(1, rows // 32, height_rows, 3)
-    for g in range(2):
-        for d in range(2):
-            relay(g, d, d, 2)
-    for d in range(2):
-        relay(2, d, 1 - d, 3)
+    @pl.when(has_prev)
+    def _():
+        gate_copy.wait_recv()
+        for c in range(cblocks):
+            r.gx[c, :HALO, :] = r.gate_in[:, c * LANES:(c + 1) * LANES].astype(F32)
+
+    @pl.when(jnp.logical_not(has_prev))
+    def _():
+        r.gx[:, :HALO, :] = jnp.zeros((cblocks, HALO, LANES), F32)
+
     tall = 128
     talls = rows // tall
     skip = HALO - reach
@@ -411,10 +416,13 @@
                 r.tapacc[c, j] = r.tapacc[c, j] + jnp.sum(both.reshape(tall // 8, 8, LANES), axis=0)
         return carry
 
-    early = 16
+    early = 4
     lax.fori_loop(0, early, tap_block, 0)
+    for g in range(2):
+        for d in range(2):
+            relay(g, d, d, 2)
     for d in range(2):
-        relay(2, d, d, 3)
+        relay(2, d, 1 - d, 3)
     lax.fori_loop(early, cblocks * talls, tap_block, 0)
     for c in range(cblocks):
         r.flat[c * per:c * per + ntaps, :] = jnp.sum(r.tapacc[c], axis=1)
@@ -423,24 +431,30 @@
                 r.rowacc[j, :, c * LANES:(c + 1) * LANES], axis=0, keepdims=True
             )
 
+    r.packed[...] = r.flat[...].astype(BF16)
+
     def piece(i):
-        return r.flat.at[pl.ds(pl.multiple_of(i * share, share), share)]
+        return r.packed.at[pl.ds(pl.multiple_of(i * share, share), share)]
 
     for i in range(1, PLANE):
         remote(
-            piece(lax.rem(spot + i, PLANE)), r.parts.at[i - 1], r.a_send, r.a_recv, in_plane(i),
+            piece(lax.rem(spot + i, PLANE)), r.parts.at[core, i - 1], r.a_send, r.a_recv.at[core], in_plane(i), 1,
         ).start()
-    for g, k in ((0, 0), (1, 0), (2, 1), (2, 7), (2, 0)):
-        product(g, k)
-    for g in range(2):
-        for d in range(2):
-            relay(g, d, 1 - d, 1)
-    for g in range(2):
-        for d in range(2):
-            relay(g, d, d, 1)
-    for g in range(2):
-        for s in range(2):
-            start_second(g, s)
+
+    @pl.when(core == 0)
+    def _():
+        remote(piece(spot), r.parts.at[0, PLANE - 1], r.a_send, r.a_recv.at[0], me, 1).start()
+
+    @pl.when(core == 1)
+    def _():
+        r.parts[1, PLANE - 1] = piece(spot)[...]
+
+    for d in range(2):
+        relay(2, d, d, 3)
+    for k in (1, 7, 0):
+        product(2, k)
+    for d in range(2):
+        relay(2, d, 1 - d, 2)
     step = 64
     steps = rows // step
 
@@ -462,29 +476,61 @@
         r.gg[at, cols] = (total * value * sig * (1.0 - sig)).astype(BF16)
         return carry
 
-    lax.fori_loop(0, 7, grad_block, 0)
-    for d in range(2):
-        relay(2, d, 1 - d, 2)
+    lax.fori_loop(0, 10, grad_block, 0)
+    for g in range(2):
+        for d in range(2):
+            relay(g, d, 1 - d, 1)
+    for g in range(2):
+        for d in range(2):
+            relay(g, d, d, 1)
+    for g in range(2):
+        for s in range(2):
+            start_second(g, s)
+    lax.fori_loop(10, 22, grad_block, 0)
     for d in range(2):
         relay(2, d, d, 2)
-    lax.fori_loop(7, 28, grad_block, 0)
-    remote(r.parts, r.parts, r.a_send, r.a_recv, me).wait_recv()
-    mine = piece(spot)[...]
-    for i in range(1, PLANE):
-        mine = mine + r.parts[i - 1]
-    r.pile[NZ - 1] = mine
-    for i in range(1, NZ):
-        remote(r.pile.at[NZ - 1], r.pile.at[i - 1], r.b_send, r.b_recv, along(axes[2], i)).start()
-    lax.fori_loop(28, 36, grad_block, 0)
+    lax.fori_loop(22, 28, grad_block, 0)
+    theirs = r.parts.at[0]
+    ours = r.parts.at[1, pl.ds(0, PLANE - 1)]
+    nearby = r.pile.at[pl.ds(0, NZ - 1)]
+    around = r.whole.at[pl.ds(0, PLANE - 1)]
+
+    @pl.when(core == 1)
+    def _():
+        remote(theirs, theirs, r.a_send, r.a_recv.at[0], me).wait_recv()
+        remote(ours, ours, r.a_send, r.a_recv.at[1], me).wait_recv()
+        for f in range(2):
+            mine = r.parts[f, 0].astype(F32)
+            for i in range(1, PLANE):
+                mine = mine + r.parts[f, i].astype(F32)
+            r.pile[NZ - 1, f] = mine.astype(BF16)
+        for i in range(1, NZ):
+            remote(r.pile.at[NZ - 1], r.pile.at[i - 1], r.b_send, r.b_recv, along(axes[2], i)).start()
+
+    lax.fori_loop(28, 38, grad_block, 0)
+    for g in range(2):
+        for s in range(2):
+            finish_second(g, s)
+        start_third(g)
     for d in range(2):
         relay(2, d, 1 - d, 1)
     for d in range(2):
         relay(2, d, d, 1)
     start_plane()
-    for g in range(2):
-        for s in range(2):
-            finish_second(g, s)
-        start_third(g)
+
+    @pl.when(core == 1)
+    def _():
+        remote(nearby, nearby, r.b_send, r.b_recv, me).wait_recv()
+        mine = r.pile[lax.rem(z + NZ - 1, NZ)].astype(F32)
+        for i in range(1, NZ):
+            mine = mine + r.pile[lax.rem(z - i + 2 * NZ - 1, NZ)].astype(F32)
+        r.final[...] = mine.astype(BF16)
+        for to in range(2):
+            for i in range(1, PLANE):
+                remote(r.final.at[to], r.whole.at[i - 1], r.c_send, r.c_recv, in_plane(i), to).start()
+        remote(r.final.at[0], r.whole.at[PLANE - 1], r.c_send, r.c_recv, me, 0).start()
+        r.whole[PLANE - 1] = mine[1].astype(BF16)
+
 
     @pl.when(has_next)
     def _():
@@ -495,19 +541,18 @@
     def _():
         r.hgx[:, rows:, :] = jnp.zeros((cblocks, HALO, LANES), F32)
 
-    lax.fori_loop(36, cblocks * steps, grad_block, 0)
-    nearby = r.pile.at[pl.ds(0, NZ - 1)]
-    remote(nearby, nearby, r.b_send, r.b_recv, me).wait_recv()
-    mine = r.pile[lax.rem(z + NZ - 1, NZ)]
-    for i in range(1, NZ):
-        mine = mine + r.pile[lax.rem(z - i + 2 * NZ - 1, NZ)]
-    r.whole[PLANE - 1] = mine.astype(BF16)
-    for i in range(1, PLANE):
-        remote(r.whole.at[PLANE - 1], r.whole.at[i - 1], r.c_send, r.c_recv, in_plane(i)).start()
+    lax.fori_loop(38, cblocks * steps, grad_block, 0)
     finish_third(0)
     finish_third(1)
-    around = r.whole.at[pl.ds(0, PLANE - 1)]
-    remote(around, around, r.c_send, r.c_recv, me).wait_recv()
+
+    @pl.when(core == 0)
+    def _():
+        remote(r.whole, r.whole, r.c_send, r.c_recv, me).wait_recv()
+
+    @pl.when(core == 1)
+    def _():
+        remote(around, around, r.c_send, r.c_recv, me).wait_recv()
+
     gains, shifts = [], []
     for c in range(cblocks):
         cols = slice(c * LANES, (c + 1) * LANES)
@@ -532,9 +577,17 @@
         remote(sent2[g], came2[g], r.second_send.at[g], r.second_recv.at[g, 0], me).wait_send()
         remote(sent3[g], came3[g], r.third_send.at[g], r.third_recv.at[g], me).wait_send()
     remote(r.sent_p, r.came_p, r.plane_send, r.plane_recv, me).wait_send()
-    remote(r.parts, r.parts, r.a_send, r.a_recv, me).wait_send()
-    remote(nearby, nearby, r.b_send, r.b_recv, me).wait_send()
-    remote(around, around, r.c_send, r.c_recv, me).wait_send()
+
+    @pl.when(core == 0)
+    def _():
+        remote(theirs, theirs, r.a_send, r.a_recv.at[0], me).wait_send()
+
+    @pl.when(core == 1)
+    def _():
+        remote(ours, ours, r.a_send, r.a_recv.at[1], me).wait_send()
+        remote(nearby, nearby, r.b_send, r.b_recv, me).wait_send()
+        remote(r.whole, r.whole, r.c_send, r.c_recv, me).wait_send()
+        remote(around, around, r.c_send, r.c_recv, me).wait_send()
 
     @pl.when(has_prev)
     def _():
@@ -566,7 +619,7 @@
     block = width // n
     cblocks = chan // LANES
     per = -(-(ntaps + 2) // 8) * 8
-    share = -(-(-(-per * cblocks // PLANE)) // 8) * 8
+    share = -(-(-(-per * cblocks // PLANE)) // 16) * 16
     hbm = pl.BlockSpec(memory_space=pl.ANY)
     vmem = pl.BlockSpec(memory_space=pltpu.VMEM)
     dma = pltpu.SemaphoreType.DMA
@@ -628,8 +681,10 @@
         sent_p=pieces(PLANE - 1),
         came_p=pieces(PLANE - 1),
         flat=pltpu.VMEM((PLANE * share, LANES), F32),
-        parts=pltpu.VMEM((PLANE - 1, share, LANES), F32),
-        pile=pltpu.VMEM((NZ, share, LANES), F32),
+        packed=pltpu.VMEM((PLANE * share, LANES), BF16),
+        parts=pltpu.VMEM((2, PLANE, share, LANES), BF16),
+        pile=pltpu.VMEM((NZ, 2, share, LANES), BF16),
+        final=pltpu.VMEM((2, share, LANES), BF16),
         whole=pltpu.VMEM((PLANE, share, LANES), BF16),
         in_sem=dma((8,)),
         tp_send=dma((2,)),
@@ -647,7 +702,7 @@
         gate_send=dma,
         gate_recv=dma,
         a_send=dma,
-        a_recv=dma,
+        a_recv=dma((2,)),
         b_send=dma,
         b_recv=dma,
         c_send=dma,

time: 39.8 us -> 38.9 us (0.977)
  the two profiles are of different devices: /device:TPU:8 before, /device:TPU:1 now
where the time goes in v4:
time: 38.9 us; the launch traced here: 38.8 us
  Pallas kernels  38.2 us (98%)
  between operations  0.64 us (2%)
    pallas_call x1, Pallas kernels, local(): pl.pallas_call(functools.partial(kernel, (*ins, *outs, *scratch)), out_sh...  36.9 us
    pallas_call x1, Pallas kernels, local(): pl.pallas_call(place, out_shape=[jax.ShapeDtypeStruct(*out) for out in ou...  1.23 us

profile of v4, /device:TPU:1, one launch (start us, length us, event | category | flops | bytes accessed | tf_op | source)
XLA Modules:
  0.0 38.8 jit_solution(3382202840253552567)
XLA Ops:
  0.6 36.9 %shard_map.127 = (bf16[512,768]{1,0:T(8,128)(2,1)S(1)}, bf16[512,768]{1,0:T(8,128)(2,1)S(1)}, f32[31,768]{1,0:T(8,128)S(1)}, f32[768]{0:T(1024)S(1)}, f32[768]{0:T(1024)S(1)}, /*index=5*/f32[16,768]{1,0:T(8,128)S(1)}) custom-call(bf16[512,768]{1,0:T(8,128)(2,1)} %refs_0_.1, bf16[512,768]{1,0:T(8,128)(2,1)} %refs_1_.1, bf16[512,768]{1,0:T(8,128)(2,1)} %refs_2_.1, ...), custom_call_target="tpu_custom_call" | custom-call | tf_op jit(solution)/shard_map/pallas_call | solution.py:720
  37.6 1.2 %shard_map.128 = (bf16[512,768]{1,0:T(8,128)(2,1)}, bf16[512,768]{1,0:T(8,128)(2,1)}, f32[31,768]{1,0:T(8,128)}, f32[768]{0:T(1024)}, f32[768]{0:T(1024)}, /*index=5*/f32[16,768]{1,0:T(8,128)}) custom-call(bf16[512,768]{1,0:T(8,128)(2,1)S(1)} %get-tuple-element.12.refs_0_, bf16[512,768]{1,0:T(8,128)(2,1)S(1)} %get-tuple-element.13.refs_1_, ...), custom_call_target="tpu_custom_call" | custom-call | tf_op jit(solution)/shard_map/pallas_call | solution.py:737

commit v5 on v4

--- a/solution.py
+++ b/solution.py
@@ -159,9 +159,6 @@
 
     repeat(0, rows // 32, gate, 2)
 
-    pl.semaphore_wait(barrier, friends)
-    swap_a = remote(r.pk_a, r.pk_b, r.tp_send.at[0], r.tp_recv.at[0], me, 1 - core)
-    swap_a.start()
     loads[1].wait()
     slab = width // NZ
 
@@ -171,6 +168,9 @@
         return carry
 
     lax.fori_loop(0, NZ, transpose, 0)
+    pl.semaphore_wait(barrier, friends)
+    swap_a = remote(r.pk_a, r.pk_b, r.tp_send.at[0], r.tp_recv.at[0], me, 1 - core)
+    swap_a.start()
     gate_copy = remote(r.gate_out, r.gate_in, r.gate_send, r.gate_recv, lax.rem(me + 1, n))
 
     @pl.when(has_next)
@@ -181,6 +181,12 @@
     loads[7].wait()
     gain = r.gain[...].reshape(1, chan)
     shift = r.shift[...].reshape(1, chan)
+    loads[2].wait()
+    def act(i):
+        cols = slice(i * gcols, (i + 1) * gcols)
+        r.scaled[:, cols] = jnp.dot(r.og[...], r.w[:, cols], preferred_element_type=F32)
+
+    act(0)
     swap_a.wait()
     gap = r.pk_a[0] - r.pk_b[0]
     variance = (r.pk_a[1] + r.pk_b[1] + gap * gap * (0.5 * chan)) / chan_total
@@ -318,11 +324,6 @@
         product(g, k)
     for g in (2, 0, 1):
         launch(g, True)
-    loads[2].wait()
-
-    def act(i):
-        cols = slice(i * gcols, (i + 1) * gcols)
-        r.scaled[:, cols] = jnp.dot(r.og[...], r.w[:, cols], preferred_element_type=F32)
 
     def grads(i):
         cols = slice(i * gcols, (i + 1) * gcols)
@@ -343,7 +344,6 @@
         for j in range(2):
             r.rowacc[j, :, cols] = sums[j]
 
-    act(0)
     for i in range(1, GROUPS):
         act(i)
         grads(i - 1)
@@ -363,10 +363,11 @@
     for c in range(cblocks):
         r.tapf[c] = r.taps[:, c * LANES:(c + 1) * LANES].astype(F32)
     r.flat[...] = jnp.zeros_like(r.flat)
-    for g, k in ((2, 2), (2, 6), (0, 0), (1, 0)):
+    for g, k in ((2, 2), (2, 6), (0, 0)):
         product(g, k)
     for d in range(2):
         relay(2, d, d, 4)
+    product(1, 0)
     swap_b.wait()
     unpack((r.pk_c[0] + r.pk_d[0]) / chan_total, r.st_a)
     unpack((r.pk_c[1] + r.pk_d[1]) / chan_total, r.st_b)
@@ -423,7 +424,11 @@
             relay(g, d, d, 2)
     for d in range(2):
         relay(2, d, 1 - d, 3)
-    lax.fori_loop(early, cblocks * talls, tap_block, 0)
+    late = 20
+    lax.fori_loop(early, late, tap_block, 0)
+    for d in range(2):
+        relay(2, d, d, 3)
+    lax.fori_loop(late, cblocks * talls, tap_block, 0)
     for c in range(cblocks):
         r.flat[c * per:c * per + ntaps, :] = jnp.sum(r.tapacc[c], axis=1)
         for j in range(2):
@@ -449,8 +454,6 @@
     def _():
         r.parts[1, PLANE - 1] = piece(spot)[...]
 
-    for d in range(2):
-        relay(2, d, d, 3)
     for k in (1, 7, 0):
         product(2, k)
     for d in range(2):
@@ -486,10 +489,10 @@
     for g in range(2):
         for s in range(2):
             start_second(g, s)
-    lax.fori_loop(10, 22, grad_block, 0)
+    lax.fori_loop(10, 20, grad_block, 0)
     for d in range(2):
         relay(2, d, d, 2)
-    lax.fori_loop(22, 28, grad_block, 0)
+    lax.fori_loop(20, 28, grad_block, 0)
     theirs = r.parts.at[0]
     ours = r.parts.at[1, pl.ds(0, PLANE - 1)]
     nearby = r.pile.at[pl.ds(0, NZ - 1)]
@@ -504,8 +507,13 @@
             for i in range(1, PLANE):
                 mine = mine + r.parts[f, i].astype(F32)
             r.pile[NZ - 1, f] = mine.astype(BF16)
-        for i in range(1, NZ):
-            remote(r.pile.at[NZ - 1], r.pile.at[i - 1], r.b_send, r.b_recv, along(axes[2], i)).start()
+        for q in range(NZ):
+
+            @pl.when(z != q)
+            def _(q=q):
+                remote(
+                    r.pile.at[NZ - 1], r.pile.at[lax.rem(q - z + 2 * NZ - 1, NZ)], r.b_send, r.b_recv, q * PLANE + spot,
+                ).start()
 
     lax.fori_loop(28, 38, grad_block, 0)
     for g in range(2):
@@ -525,10 +533,15 @@
         for i in range(1, NZ):
             mine = mine + r.pile[lax.rem(z - i + 2 * NZ - 1, NZ)].astype(F32)
         r.final[...] = mine.astype(BF16)
-        for to in range(2):
-            for i in range(1, PLANE):
-                remote(r.final.at[to], r.whole.at[i - 1], r.c_send, r.c_recv, in_plane(i), to).start()
-        remote(r.final.at[0], r.whole.at[PLANE - 1], r.c_send, r.c_recv, me, 0).start()
+        for q in range(PLANE):
+            goes = r.whole.at[lax.rem(q - spot + 2 * PLANE - 1, PLANE)]
+
+            @pl.when(spot != q)
+            def _(q=q, goes=goes):
+                remote(r.final.at[1], goes, r.c_send, r.c_recv, me - spot + q, 1).start()
+
+            remote(r.final.at[0], goes, r.c_send, r.c_recv, me - spot + q, 0).start()
+
         r.whole[PLANE - 1] = mine[1].astype(BF16)
 
 

time: 38.9 us -> 38.3 us (0.985)
  the two profiles are of different devices: /device:TPU:1 before, /device:TPU:8 now
where the time goes in v5:
time: 38.3 us; the launch traced here: 37.6 us
  Pallas kernels  36.9 us (96%)
  between operations  0.64 us (2%)
    pallas_call x1, Pallas kernels, local(): pl.pallas_call(functools.partial(kernel, (*ins, *outs, *scratch)), out_sh...  35.7 us
    pallas_call x1, Pallas kernels, local(): pl.pallas_call(place, out_shape=[jax.ShapeDtypeStruct(*out) for out in ou...  1.23 us

profile of v5, /device:TPU:8, one launch (start us, length us, event | category | flops | bytes accessed | tf_op | source)
XLA Modules:
  0.0 37.6 jit_solution(12237300628180478103)
XLA Ops:
  0.6 35.7 %shard_map.127 = (bf16[512,768]{1,0:T(8,128)(2,1)S(1)}, bf16[512,768]{1,0:T(8,128)(2,1)S(1)}, f32[31,768]{1,0:T(8,128)S(1)}, f32[768]{0:T(1024)S(1)}, f32[768]{0:T(1024)S(1)}, /*index=5*/f32[16,768]{1,0:T(8,128)S(1)}) custom-call(bf16[512,768]{1,0:T(8,128)(2,1)} %refs_0_.1, bf16[512,768]{1,0:T(8,128)(2,1)} %refs_1_.1, bf16[512,768]{1,0:T(8,128)(2,1)} %refs_2_.1, ...), custom_call_target="tpu_custom_call" | custom-call | tf_op jit(solution)/shard_map/pallas_call | solution.py:733
  36.4 1.2 %shard_map.128 = (bf16[512,768]{1,0:T(8,128)(2,1)}, bf16[512,768]{1,0:T(8,128)(2,1)}, f32[31,768]{1,0:T(8,128)}, f32[768]{0:T(1024)}, f32[768]{0:T(1024)}, /*index=5*/f32[16,768]{1,0:T(8,128)}) custom-call(bf16[512,768]{1,0:T(8,128)(2,1)S(1)} %get-tuple-element.12.refs_0_, bf16[512,768]{1,0:T(8,128)(2,1)S(1)} %get-tuple-element.13.refs_1_, ...), custom_call_target="tpu_custom_call" | custom-call | tf_op jit(solution)/shard_map/pallas_call | solution.py:750
